TPU v7x, 512 devices: a whole 4x4x16 slice. The times are simulated.
512 devices in a mesh: sp: 16 (over z), fs: 4 (over y), tp: 8 (over x, core).
Axes of the slice: x: 4, y: 4, z: 16, core: 2. Of those that a mesh axis runs over, the one named last changes fastest.
Arguments:
- tokens: bfloat16 [32768, 2048], P(('fs', 'sp')), parts along dimension 0, may hold values from -6 to 6
- norm_gain: float32 [2048], replicated, may hold values from 0.1 to 1.9
- state_gate: bfloat16 [2048, 1024], P('sp', 'tp'), may hold values from -0.125 to 0.125
- state_value: bfloat16 [2048, 1024], P('sp', 'tp'), may hold values from -0.125 to 0.125
- state_keys: bfloat16 [2048, 1024], P('sp', 'tp'), may hold values from -0.125 to 0.125
- state_query: bfloat16 [2048, 1024], P('sp', 'tp'), may hold values from -0.125 to 0.125
- state_step: bfloat16 [2048, 16], replicated, may hold values from -0.125 to 0.125
- state_rate: float32 [16], P('tp'), may hold values from 0 to 1, as said below
- state_jumps: float32 [32768, 16], P(('fs', 'sp'), 'tp'), parts along dimension 0, may hold values from -3 to 0
- state_gain: float32 [1024], P('tp'), may hold values from 0.1 to 1.9
- filter_value: bfloat16 [5, 1024], P(None, 'tp'), may hold values from -2.5 to 2.5
- filter_keys: bfloat16 [5, 1024], P(None, 'tp'), may hold values from -2.5 to 2.5
- filter_query: bfloat16 [5, 1024], P(None, 'tp'), may hold values from -2.5 to 2.5
- window_query: bfloat16 [2048, 2048], P('sp', 'tp'), may hold values from -64 to 64
- window_keys: bfloat16 [2048, 1024], P('sp', 'tp'), may hold values from -1 to 1
- window_values: bfloat16 [2048, 1024], P('sp', 'tp'), may hold values from -0.125 to 0.125
- window_sink: float32 [16], P('tp'), may hold values from 2.5 to 5.5
- state_output: bfloat16 [1024, 2048], P('tp', 'sp'), may hold values from -0.1875 to 0.1875
- window_output: bfloat16 [2048, 2048], P('tp', 'sp'), may hold values from -2 to 2
Outputs:
- mixed: bfloat16 [32768, 2048], P(('fs', 'sp', 'tp')), parts along dimension 0
There are 4 independent parts, one for each index of `fs`. A program takes and returns all parts, laid end to end along the dimension named above; an argument that names none is the same for every part. Nothing has to cross between parts.
Inputs may be any that keep to these rules, and one draw needn't show every extreme that they name: `state_rate`: a positive rate for each head.
All inputs are finite; a program needn't handle non-finite values.
Results may differ from a plain program's by a relative error of at most 0.015.
The roundings to bfloat16 on the way count: a program that leaves them out, or rounds other values in their place, can miss the bound.
Values may be sent and summed in bfloat16 or wider, within the bound.
A program may use at most 64 MiB of HBM per device.

v0:
```python
import jax
import jax.numpy as jnp
from jax import lax
from jax.sharding import PartitionSpec as P

STATE_SIZE = 128
HEAD_DIM = 128
WINDOW = 128
BLOCK = 128
GRID_WIDTH = 64


def turned_gather(arrays, axis, dims):
    turned = [jnp.moveaxis(a, dim, 0) for a, dim in zip(arrays, dims)]
    widths = [t[0].size for t in turned]
    both = jnp.concatenate([t.reshape(-1, w) for t, w in zip(turned, widths)], axis=1)
    out = lax.all_gather(both, axis, axis=0, tiled=True)
    pieces = jnp.split(out, [sum(widths[:k]) for k in range(1, len(widths))], axis=1)
    return tuple(
        (
            jnp.moveaxis(b.reshape(-1, *t.shape[1:]), 0, dim)
            for b, t, dim in zip(pieces, turned, dims)
        )
    )


def extended(cells, sides, width):
    for axis, dim in sides:
        count = lax.axis_size(axis)
        ends = count - 1
        head = lax.slice_in_dim(cells, 0, width, axis=dim)
        tail = lax.slice_in_dim(cells, cells.shape[dim] - width, cells.shape[dim], axis=dim)
        cells = jnp.concatenate(
            [
                lax.ppermute(tail, axis, [(i, (i + 1) % count) for i in range(ends)]),
                cells,
                lax.ppermute(head, axis, [((i + 1) % count, i) for i in range(ends)]),
            ],
            axis=dim,
        )
    return cells


def split_up(value, dim, length):
    lengths = value.shape
    pieces = value.reshape(*lengths[:dim], length, lengths[dim] // length, *lengths[dim + 1 :])
    return jnp.moveaxis(pieces, dim, 0)


def summed_on_arrival(value, axis, dim):
    pieces = split_up(value, dim, lax.axis_size(axis))
    arrived = lax.all_to_all(pieces, axis, split_axis=0, concat_axis=0, tiled=True)
    return arrived.astype(jnp.float32).sum(axis=0)


def rotate_grid(vectors, positions, grid_width):
    head_dim = vectors.shape[-1]
    quarter = head_dim // 4
    half_dim = head_dim // 2
    inverse = 10000.0 ** (-jnp.arange(quarter, dtype=jnp.float32) / quarter)
    grid_row = (positions // grid_width).astype(jnp.float32)
    grid_col = (positions % grid_width).astype(jnp.float32)
    angle_row = grid_row[:, None] * inverse[None, :]
    angle_col = grid_col[:, None] * inverse[None, :]
    angles = jnp.concatenate([angle_row, angle_row, angle_col, angle_col], axis=-1)[:, None, :]
    first_half = vectors[..., :half_dim]
    second = vectors[..., half_dim:]
    turned = jnp.concatenate(
        [
            -first_half[..., quarter:],
            first_half[..., :quarter],
            -second[..., quarter:],
            second[..., :quarter],
        ],
        axis=-1,
    )
    return (
        vectors.astype(jnp.float32) * jnp.cos(angles) + turned.astype(jnp.float32) * jnp.sin(angles)
    ).astype(jnp.bfloat16)


def window_attend(query_rows, keys_pad, values_pad, sink_logits, key_start, total_len, window):
    row_count, query_heads, head_dim = query_rows.shape
    kv_heads = keys_pad.shape[1]
    group_size = query_heads // kv_heads
    block_count = row_count // window
    query_blocks = query_rows.reshape(block_count, window, kv_heads, group_size, head_dim)
    key_split = keys_pad.reshape(block_count + 2, window, kv_heads, head_dim)
    value_split = values_pad.reshape(block_count + 2, window, kv_heads, head_dim)
    key_band = jnp.concatenate([key_split[:-2], key_split[1:-1], key_split[2:]], axis=1)
    value_band = jnp.concatenate([value_split[:-2], value_split[1:-1], value_split[2:]], axis=1)
    scores = jnp.einsum(
        "kihgd,kjhd->khgij", query_blocks, key_band, preferred_element_type=jnp.float32
    ) * head_dim ** (-0.5)
    query_pos = jnp.arange(window)[:, None]
    band_pos = jnp.arange(3 * window)[None, :]
    within = jnp.abs(band_pos - window - query_pos) <= window
    key_pos = (
        key_start + jnp.arange(block_count)[:, None] * window + jnp.arange(3 * window)[None, :]
    )
    inside = (key_pos >= 0) & (key_pos < total_len)
    valid_pair = (within[None] & inside[:, None, :])[:, None, None]
    sink_logit = sink_logits.reshape(kv_heads, group_size)[None, :, :, None, None]
    masked = jnp.where(valid_pair, scores, -1e30)
    ceiling = jnp.maximum(jnp.max(masked, axis=-1, keepdims=True), sink_logit)
    weights = jnp.where(valid_pair, jnp.exp(masked - ceiling), 0.0)
    denominator = jnp.exp(sink_logit - ceiling) + jnp.sum(weights, axis=-1, keepdims=True)
    weights_bf = (weights / denominator).astype(jnp.bfloat16)
    mixed_rows = jnp.einsum(
        "khgij,kjhd->kihgd", weights_bf, value_band, preferred_element_type=jnp.float32
    )
    return mixed_rows.reshape(row_count, query_heads * head_dim).astype(jnp.bfloat16)


def block_terms(query_rows, key_rows, value_rows, log_rows, block_len):
    row_count, group_count, state_size = query_rows.shape
    head_ratio, head_dim = (value_rows.shape[2], value_rows.shape[3])
    block_count = row_count // block_len
    query_blocks = query_rows.reshape(block_count, block_len, group_count, state_size)
    key_blocks = key_rows.reshape(block_count, block_len, group_count, state_size)
    value_blocks = value_rows.reshape(block_count, block_len, group_count, head_ratio, head_dim)
    decay_cum = jnp.cumsum(
        log_rows.reshape(block_count, block_len, group_count, head_ratio), axis=1
    )
    decay_total = decay_cum[:, -1]
    gram_block = jnp.einsum(
        "kign,kjgn->kgij", query_blocks, key_blocks, preferred_element_type=jnp.float32
    )
    cum_heads = jnp.moveaxis(decay_cum, 1, 3)
    distance = jnp.abs(cum_heads[..., :, None] - cum_heads[..., None, :])
    pair_weight = (gram_block[:, :, None] * jnp.exp(-distance)).astype(jnp.bfloat16)
    near_terms = jnp.einsum(
        "kgrij,kjgrp->kigrp", pair_weight, value_blocks, preferred_element_type=jnp.float32
    )
    keys_after = (
        key_blocks[:, :, :, None, :] * jnp.exp(decay_total[:, None] - decay_cum)[..., None]
    ).astype(jnp.bfloat16)
    keys_before = (key_blocks[:, :, :, None, :] * jnp.exp(decay_cum)[..., None]).astype(
        jnp.bfloat16
    )
    state_after = jnp.einsum(
        "kjgrn,kjgrp->kgrnp", keys_after, value_blocks, preferred_element_type=jnp.float32
    )
    state_before = jnp.einsum(
        "kjgrn,kjgrp->kgrnp", keys_before, value_blocks, preferred_element_type=jnp.float32
    )
    before = jnp.cumsum(decay_total, axis=0) - decay_total
    overall = jnp.sum(decay_total, axis=0)
    after_sum = overall[None] - before - decay_total
    block_order = jnp.arange(block_count)
    earlier_mask = (block_order[None, :] < block_order[:, None])[:, :, None, None]
    later_mask = (block_order[None, :] > block_order[:, None])[:, :, None, None]
    gap_fwd = before[:, None] - before[None, :] - decay_total[None, :]
    gap_bwd = before[None, :] - before[:, None] - decay_total[:, None]
    weight_fwd = jnp.where(earlier_mask, jnp.exp(jnp.minimum(gap_fwd, 0.0)), 0.0)
    weight_bwd = jnp.where(later_mask, jnp.exp(jnp.minimum(gap_bwd, 0.0)), 0.0)
    carried_fwd = jnp.einsum("abgr,bgrnp->agrnp", weight_fwd, state_after)
    carried_bwd = jnp.einsum("abgr,bgrnp->agrnp", weight_bwd, state_before)
    summary_fwd = jnp.einsum("agr,agrnp->grnp", jnp.exp(after_sum), state_after)
    summary_bwd = jnp.einsum("agr,agrnp->grnp", jnp.exp(before), state_before)
    pieces = (
        near_terms,
        carried_fwd,
        carried_bwd,
        decay_cum,
        decay_total,
        before,
        after_sum,
        query_blocks,
    )
    return (pieces, (summary_fwd, summary_bwd, overall))


def finish_terms(pieces, incoming_fwd, incoming_bwd):
    (
        near_terms,
        carried_fwd,
        carried_bwd,
        decay_cum,
        decay_total,
        before,
        after_sum,
        query_blocks,
    ) = pieces
    total_fwd = carried_fwd + jnp.exp(before)[..., None, None] * incoming_fwd[None]
    total_bwd = carried_bwd + jnp.exp(after_sum)[..., None, None] * incoming_bwd[None]
    query_wide = query_blocks.astype(jnp.float32)
    read_fwd = jnp.einsum("kign,kgrnp->kigrp", query_wide, total_fwd)
    read_bwd = jnp.einsum("kign,kgrnp->kigrp", query_wide, total_bwd)
    combined = (
        near_terms
        + jnp.exp(decay_cum)[..., None] * read_fwd
        + jnp.exp(decay_total[:, None] - decay_cum)[..., None] * read_bwd
    )
    block_count, block_len, group_count, head_ratio, head_dim = combined.shape
    return combined.reshape(block_count * block_len, group_count, head_ratio, head_dim)


def combine_all(gathered_states, own_index):
    after_all, before_all, logs_all = gathered_states
    device_count = logs_all.shape[0]
    cum_incl = jnp.cumsum(logs_all, axis=0)
    cum_excl = cum_incl - logs_all
    device_order = jnp.arange(device_count)
    picker = (device_order == own_index).astype(jnp.float32)[:, None, None]
    own_incl = jnp.sum(picker * cum_incl, axis=0)
    own_excl = jnp.sum(picker * cum_excl, axis=0)
    lower_mask = (device_order < own_index)[:, None, None]
    higher_mask = (device_order > own_index)[:, None, None]
    weight_fwd = jnp.where(lower_mask, jnp.exp(jnp.minimum(own_excl[None] - cum_incl, 0.0)), 0.0)
    weight_bwd = jnp.where(higher_mask, jnp.exp(jnp.minimum(cum_excl - own_incl[None], 0.0)), 0.0)
    incoming_fwd = jnp.einsum("dgr,dgrnp->grnp", weight_fwd, after_all)
    incoming_bwd = jnp.einsum("dgr,dgrnp->grnp", weight_bwd, before_all)
    return (incoming_fwd, incoming_bwd)


def shards(
    tokens,
    norm_gain,
    state_gate,
    state_value,
    state_keys,
    state_query,
    state_step,
    state_rate,
    state_jumps,
    state_gain,
    filter_value,
    filter_keys,
    filter_query,
    window_query,
    window_keys,
    window_values,
    window_sink,
    state_output,
    window_output,
):
    row_count = tokens.shape[0]
    rows_wide = tokens.astype(jnp.float32)
    normed = (
        rows_wide
        * lax.rsqrt(jnp.mean(rows_wide * rows_wide, axis=-1, keepdims=True) + 1e-06)
        * norm_gain
    ).astype(jnp.bfloat16)
    gathered = turned_gather(
        (
            state_gate,
            state_value,
            state_keys,
            state_query,
            window_query,
            window_keys,
            window_values,
            state_output,
            window_output,
        ),
        "sp",
        (0, 0, 0, 0, 0, 0, 0, 1, 1),
    )
    projected = [
        jnp.dot(normed, matrix, preferred_element_type=jnp.float32) for matrix in gathered[:7]
    ]
    out_state = gathered[7]
    out_window = gathered[8]
    gate_rows, value_pre, keys_pre, query_pre, query_raw, keys_raw, values_rows = [
        result.astype(jnp.bfloat16) for result in projected
    ]
    head_local = state_rate.shape[0]
    group_local = keys_pre.shape[1] // STATE_SIZE
    head_dim = value_pre.shape[1] // head_local
    head_ratio = head_local // group_local
    step_cols = lax.dynamic_slice_in_dim(
        state_step, lax.axis_index("tp") * head_local, head_local, 1
    )
    step_rows = jax.nn.softplus(jnp.dot(normed, step_cols, preferred_element_type=jnp.float32))
    log_decay = -state_rate[None, :] * step_rows + state_jumps
    half_width = filter_value.shape[0] // 2
    stacked = jnp.concatenate([value_pre, keys_pre, query_pre], axis=-1)
    padded = extended(stacked, (("sp", 0),), half_width)
    filters = jnp.concatenate([filter_value, filter_keys, filter_query], axis=-1).astype(
        jnp.float32
    )
    filtered = jnp.zeros(stacked.shape, jnp.float32)
    for offset in range(filters.shape[0]):
        filtered = (
            filtered + padded[offset : offset + row_count].astype(jnp.float32) * filters[offset]
        )
    value_cols = value_pre.shape[1]
    key_cols = keys_pre.shape[1]
    inner_rows = (
        jax.nn.silu(filtered[:, :value_cols]).reshape(row_count, head_local, head_dim)
        * step_rows[..., None]
    )
    scan_values = inner_rows.astype(jnp.bfloat16).reshape(
        row_count, group_local, head_ratio, head_dim
    )
    scan_keys = (
        filtered[:, value_cols : value_cols + key_cols]
        .astype(jnp.bfloat16)
        .reshape(row_count, group_local, STATE_SIZE)
    )
    scan_query = (
        filtered[:, value_cols + key_cols :]
        .astype(jnp.bfloat16)
        .reshape(row_count, group_local, STATE_SIZE)
    )
    pieces, summaries = block_terms(
        scan_query,
        scan_keys,
        scan_values,
        log_decay.reshape(row_count, group_local, head_ratio),
        BLOCK,
    )
    summary_fwd, summary_bwd, overall = summaries
    gathered_states = (
        lax.all_gather(summary_fwd[None].astype(jnp.bfloat16), "sp", axis=0, tiled=True).astype(
            jnp.float32
        ),
        lax.all_gather(summary_bwd[None].astype(jnp.bfloat16), "sp", axis=0, tiled=True).astype(
            jnp.float32
        ),
        lax.all_gather(overall[None].astype(jnp.bfloat16), "sp", axis=0, tiled=True).astype(
            jnp.float32
        ),
    )
    incoming_fwd, incoming_bwd = combine_all(gathered_states, lax.axis_index("sp"))
    scan_out = finish_terms(pieces, incoming_fwd, incoming_bwd).reshape(
        row_count, head_local * head_dim
    )
    gated_rows = scan_out * jax.nn.silu(gate_rows.astype(jnp.float32))
    per_head = gated_rows.reshape(row_count, head_local, head_dim)
    state_mix = (
        (
            per_head
            * lax.rsqrt(jnp.mean(per_head * per_head, axis=-1, keepdims=True) + 1e-06)
            * state_gain.reshape(head_local, head_dim)
        )
        .astype(jnp.bfloat16)
        .reshape(row_count, head_local * head_dim)
    )
    query_heads = window_sink.shape[0]
    kv_heads = keys_raw.shape[1] // HEAD_DIM
    kv_width = kv_heads * HEAD_DIM
    positions = lax.axis_index("sp") * row_count + jnp.arange(row_count, dtype=jnp.int32)
    query_rot = rotate_grid(
        query_raw.reshape(row_count, query_heads, HEAD_DIM), positions, GRID_WIDTH
    )
    keys_rot = rotate_grid(keys_raw.reshape(row_count, kv_heads, HEAD_DIM), positions, GRID_WIDTH)
    pair_rows = jnp.concatenate([keys_rot.reshape(row_count, kv_width), values_rows], axis=-1)
    padded_pair = extended(pair_rows, (("sp", 0),), WINDOW)
    keys_pad = padded_pair[:, :kv_width].reshape(-1, kv_heads, HEAD_DIM)
    values_pad = padded_pair[:, kv_width:].reshape(-1, kv_heads, HEAD_DIM)
    window_mix = window_attend(
        query_rot,
        keys_pad,
        values_pad,
        window_sink,
        lax.axis_index("sp") * row_count - WINDOW,
        lax.axis_size("sp") * row_count,
        WINDOW,
    )
    summed = summed_on_arrival(
        (
            jnp.dot(state_mix, out_state, preferred_element_type=jnp.float32)
            + jnp.dot(window_mix, out_window, preferred_element_type=jnp.float32)
        ).astype(jnp.bfloat16),
        "tp",
        0,
    )
    return summed.astype(jnp.bfloat16)


def solution(mesh):
    placed = (
        P(("fs", "sp"), None),
        P(),
        P("sp", "tp"),
        P("sp", "tp"),
        P("sp", "tp"),
        P("sp", "tp"),
        P(),
        P("tp"),
        P(("fs", "sp"), "tp"),
        P("tp"),
        P(None, "tp"),
        P(None, "tp"),
        P(None, "tp"),
        P("sp", "tp"),
        P("sp", "tp"),
        P("sp", "tp"),
        P("tp"),
        P("tp", "sp"),
        P("tp", "sp"),
    )
    return jax.shard_map(
        shards, mesh=mesh, in_specs=placed, out_specs=P(("fs", "sp", "tp"), None), check_vma=False
    )
```

profile of v0, /device:TPU:1, one launch (start us, length us, event | category | flops | bytes accessed | tf_op | source)
XLA Modules:
  0.0 283.0 jit_solution(2095832873508583214)
XLA Ops:
  6.5 1.0 copy.150
  7.6 0.9 copy.151
  8.4 0.9 copy.152
  9.3 0.9 copy.153
  10.2 0.9 copy.155
  11.1 0.9 copy.156
  11.9 1.0 copy.154
  13.0 0.8 bitcast_dynamic-update-slice_fusion.1
  13.8 0.9 bitcast_dynamic-update-slice_fusion
  14.7 0.8 copy-done.13
  15.4 0.7 neg.49
  16.1 2.1 fusion
  18.8 1.3 copy-done.2
  20.1 1.3 multiply_add_fusion.1
  22.2 0.6 subtract_exponential_fusion
  23.5 1.3 dynamic-slice
  25.7 31.4 %all-reduce = bf16[32]{0:T(256)(128)(2,1)S(1)} all-reduce(bf16[32]{0:T(256)(128)(2,1)S(1)} %dynamic-update-slice), channel_id=2, replica_groups=mesh['sp'=16,'fs'=4,'tp'=8] {'sp'}, use_global_device_ids=true, to_apply=%add | all-reduce | flops 32 | bytes 128
  57.5 0.6 copy.178
  58.2 0.6 convert_reduce_fusion.3
  58.8 0.6 iota_compare_fusion.1
  59.4 0.6 iota_compare_fusion
  60.1 2.8 fusion.69
  63.0 0.6 fusion.116
  63.6 0.6 fusion.115
  64.4 1.0 broadcast_and_fusion
  65.4 52.4 %all-gather.5.cloned.1.call-done = bf16[2048,1408]{0,1:T(8,128)(2,1)} async-done(((bf16[128,1408]{0,1:T(8,128)(2,1)}), bf16[2048,1408]{0,1:T(8,128)(2,1)}) %all-gather.5.cloned.1.call-update) | async-done | bytes 5767184 | tf_op jit(solution)/shard_map/all_gather | solution.py:17
  117.7 1.9 convolution_convert_fusion.2
  119.7 0.7 copy.184
  120.3 1.9 convolution_convert_fusion.3
  122.2 1.0 add_convert_fusion.2
  123.3 0.7 pad_maximum_fusion.11
  123.9 3.9 %collective-permute-start.2 = (bf16[128,256]{0,1:T(8,128)(2,1)}, bf16[128,256]{0,1:T(8,128)(2,1)}, u32[]{:S(2)}, u32[]{:S(2)}) collective-permute-start(bf16[128,256]{0,1:T(8,128)(2,1)} %get-tuple-element.36), channel_id=1, source_target_pairs={{0,32},{32,64},{64,96},{96,128},{128,160},{160,192},{192,224},{224... | collective-permute-start | bytes 196616 | tf_op jit(solution)/shard_map/ppermute | solution.py:35
  127.8 2.0 convolution_convert_fusion.1
  130.0 0.7 concatenate.93
  130.7 1.9 convolution_convert_fusion.5
  132.6 1.9 convolution_convert_fusion.6
  134.6 1.9 convolution_convert_fusion.7
  136.6 0.7 fusion.124
  137.3 3.9 %collective-permute-start = (bf16[2,384]{0,1:T(8,128)(2,1)}, bf16[2,384]{0,1:T(8,128)(2,1)}, u32[]{:S(2)}, u32[]{:S(2)}) collective-permute-start(bf16[2,384]{0,1:T(8,128)(2,1)} %get-tuple-element.22), channel_id=1, source_target_pairs={{0,32},{32,64},{64,96},{96,128},{128,160},{160,192},{192,224},{224... | collective-permute-start | bytes 4616 | tf_op jit(solution)/shard_map/ppermute | solution.py:35
  141.2 1.3 collective-permute-start.1
  142.5 0.9 add_convert_fusion.1
  143.4 0.8 copy.216
  144.2 1.5 collective-permute-start.3
  145.6 1.2 collective-permute-done.1
  146.8 1.2 maximum_maximum_fusion
  148.0 2.0 fusion.123
  150.0 0.8 slice_bitcast_fusion.3
  150.8 0.7 reshape.688
  151.5 1.0 copy.166
  152.5 1.6 reshape.687
  154.2 1.7 copy.198
  155.8 0.8 divide_multiply_fusion
  156.6 1.0 reshape.686
  157.7 0.7 fusion.47
  159.1 0.8 fusion.57
  160.0 0.8 fusion.60
  160.8 24.8 %all-gather.1 = bf16[32,128,64]{1,2,0:T(8,128)(2,1)S(1)} all-gather(bf16[2,128,64]{1,2,0:T(8,128)(2,1)S(1)} %convert_element_type.218), channel_id=3, replica_groups=mesh['sp'=16,'fs'=4,'tp'=8] {'sp'}, dimensions={0}, use_global_device_ids=true | all-gather | bytes 557056 | tf_op jit(solution)/shard_map/all_gather | solution.py:316
  185.6 23.2 %all-gather.2 = bf16[32,128,64]{1,2,0:T(8,128)(2,1)S(1)} all-gather(bf16[2,128,64]{1,2,0:T(8,128)(2,1)S(1)} %convert_element_type.221), channel_id=4, replica_groups=mesh['sp'=16,'fs'=4,'tp'=8] {'sp'}, dimensions={0}, use_global_device_ids=true | all-gather | bytes 557056 | tf_op jit(solution)/shard_map/all_gather | solution.py:319
  211.5 2.0 bitcast_reduce_fusion
  213.6 0.9 pad_maximum_fusion.9
  216.6 1.9 fusion.14
  218.5 1.8 add_convert_fusion
  220.3 54.8 %all_to_all.5 = bf16[8,64,2048]{2,1,0:T(8,128)(2,1)S(1)} all-to-all(bf16[8,64,2048]{2,1,0:T(8,128)(2,1)S(1)} %bitcast.230), channel_id=1, replica_groups=mesh['sp'=16,'fs'=4,'tp'=8] {'tp'}, dimensions={0} | all-to-all | bytes 4194304 | tf_op jit(solution)/shard_map/all_to_all | solution.py:52
  275.1 1.1 reduce_sum.72
  (145 shorter events, 9.0 us)
Async XLA Ops:
  6.5 13.6 %copy-start = (bf16[2048,16]{0,1:T(8,128)(2,1)S(1)}, bf16[2048,16]{0,1:T(8,128)(2,1)}, u32[]{:S(2)}) copy-start(bf16[2048,16]{0,1:T(8,128)(2,1)} %param.25) | copy-start | bytes 196612
  6.5 11.6 %copy-start.1 = (bf16[512,2048]{1,0:T(8,128)(2,1)S(1)}, bf16[512,2048]{1,0:T(8,128)(2,1)}, u32[]{:S(2)}) copy-start(bf16[512,2048]{1,0:T(8,128)(2,1)} %param.19) | copy-start | bytes 6291460
  6.5 11.7 %copy-start.18 = (f32[2048]{0:T(1024)S(1)}, f32[2048]{0:T(1024)}, u32[]{:S(2)}) copy-start(f32[2048]{0:T(1024)} %param.20) | copy-start | bytes 24580
  6.5 111.2 %all-gather.5.cloned.1.call-start = ((), (), s32[]{:S(2)}) async-start(), calls=%async_computation.1 | async-start | bytes 6127616 | tf_op jit(solution)/shard_map/all_gather | solution.py:17
  14.6 0.8 copy-start.13
  18.2 1.9 copy-start.19
  18.8 1.3 copy-start.2
  20.1 38.1 %copy-start.25 = (bf16[5,128]{1,0:T(8,128)(2,1)S(1)}, bf16[5,128]{1,0:T(8,128)(2,1)}, u32[]{:S(2)}) copy-start(bf16[5,128]{1,0:T(8,128)(2,1)} %param.31) | copy-start | bytes 3844
  20.1 38.1 %copy-start.26 = (bf16[5,128]{1,0:T(8,128)(2,1)S(1)}, bf16[5,128]{1,0:T(8,128)(2,1)}, u32[]{:S(2)}) copy-start(bf16[5,128]{1,0:T(8,128)(2,1)} %param.30) | copy-start | bytes 3844
  20.1 38.1 %copy-start.27 = (bf16[5,128]{1,0:T(8,128)(2,1)S(1)}, bf16[5,128]{1,0:T(8,128)(2,1)}, u32[]{:S(2)}) copy-start(bf16[5,128]{1,0:T(8,128)(2,1)} %param.29) | copy-start | bytes 3844
  21.4 96.4 %copy-start.3 = (bf16[512,2048]{1,0:T(8,128)(2,1)S(1)}, bf16[512,2048]{1,0:T(8,128)(2,1)}, u32[]{:S(2)}) copy-start(bf16[512,2048]{1,0:T(8,128)(2,1)} %copy-done.2) | copy-start | bytes 6291460
  22.8 0.6 copy-start.22
  123.9 89.7 %collective-permute-start.2 = (bf16[128,256]{0,1:T(8,128)(2,1)}, bf16[128,256]{0,1:T(8,128)(2,1)}, u32[]{:S(2)}, u32[]{:S(2)}) collective-permute-start(bf16[128,256]{0,1:T(8,128)(2,1)} %get-tuple-element.36), channel_id=1, source_target_pairs={{0,32},{32,64},{64,96},{96,128},{128,160},{160,192},{192,224},{224... | collective-permute-start | bytes 196616 | tf_op jit(solution)/shard_map/ppermute | solution.py:35
  132.6 14.2 %copy-start.5 = (bf16[512,128]{0,1:T(8,128)(2,1)}, bf16[512,128]{0,1:T(8,128)(2,1)S(1)}, u32[]{:S(2)}) copy-start(bf16[512,128]{0,1:T(8,128)(2,1)S(1)} %convolution_convert_fusion.5) | copy-start | bytes 393220
  134.5 12.3 %copy-start.6 = (bf16[512,128]{0,1:T(8,128)(2,1)}, bf16[512,128]{0,1:T(8,128)(2,1)S(1)}, u32[]{:S(2)}) copy-start(bf16[512,128]{0,1:T(8,128)(2,1)S(1)} %convolution_convert_fusion.6) | copy-start | bytes 393220
  134.5 7.9 %copy-start.8 = (f32[4,128,128]{1,0,2:T(4,128)S(1)}, f32[4,128,128]{1,0,2:T(4,128)}, u32[]{:S(2)}) copy-start(f32[4,128,128]{1,0,2:T(4,128)} %get-tuple-element.38) | copy-start | bytes 786436
  134.5 7.9 %copy-start.9 = (f32[4,128,128]{1,0,2:T(4,128)S(1)}, f32[4,128,128]{1,0,2:T(4,128)}, u32[]{:S(2)}) copy-start(f32[4,128,128]{1,0,2:T(4,128)} %get-tuple-element.39) | copy-start | bytes 786436
  134.6 7.9 %copy-start.14 = (bf16[4,128,2,32]{1,0,3,2:T(4,128)(2,1)S(1)}, bf16[4,128,2,32]{1,0,3,2:T(4,128)(2,1)}, u32[]{:S(2)}) copy-start(bf16[4,128,2,32]{1,0,3,2:T(4,128)(2,1)} %concatenate.93) | copy-start | bytes 196612
  136.5 11.5 %copy-start.7 = (bf16[512,128]{0,1:T(8,128)(2,1)}, bf16[512,128]{0,1:T(8,128)(2,1)S(1)}, u32[]{:S(2)}) copy-start(bf16[512,128]{0,1:T(8,128)(2,1)S(1)} %convolution_convert_fusion.7) | copy-start | bytes 393220
  137.3 8.3 %collective-permute-start = (bf16[2,384]{0,1:T(8,128)(2,1)}, bf16[2,384]{0,1:T(8,128)(2,1)}, u32[]{:S(2)}, u32[]{:S(2)}) collective-permute-start(bf16[2,384]{0,1:T(8,128)(2,1)} %get-tuple-element.22), channel_id=1, source_target_pairs={{0,32},{32,64},{64,96},{96,128},{128,160},{160,192},{192,224},{224... | collective-permute-start | bytes 4616 | tf_op jit(solution)/shard_map/ppermute | solution.py:35
  141.2 5.7 %collective-permute-start.1 = (bf16[2,384]{0,1:T(8,128)(2,1)}, bf16[2,384]{0,1:T(8,128)(2,1)}, u32[]{:S(2)}, u32[]{:S(2)}) collective-permute-start(bf16[2,384]{0,1:T(8,128)(2,1)} %get-tuple-element.23), channel_id=1, source_target_pairs={{32,0},{64,32},{96,64},{128,96},{160,128},{192,160},{224,192},{256... | collective-permute-start | bytes 4616 | tf_op jit(solution)/shard_map/ppermute | solution.py:37
  144.2 69.5 %collective-permute-start.3 = (bf16[128,256]{0,1:T(8,128)(2,1)}, bf16[128,256]{0,1:T(8,128)(2,1)S(1)}, u32[]{:S(2)}, u32[]{:S(2)}) collective-permute-start(bf16[128,256]{0,1:T(8,128)(2,1)} %get-tuple-element.37), channel_id=1, source_target_pairs={{32,0},{64,32},{96,64},{128,96},{160,128},{192,160},{224,192},{256... | collective-permute-start | bytes 196616 | tf_op jit(solution)/shard_map/ppermute | solution.py:37
  156.6 52.2 %copy-start.21 = (f32[16,2]{0,1:T(2,128)S(1)}, f32[16,2]{0,1:T(2,128)}, u32[]{:S(2)}) copy-start(f32[16,2]{0,1:T(2,128)} %fusion.115) | copy-start | bytes 388
  156.6 52.6 %copy-start.23 = (f32[4,2]{0,1:T(2,128)S(1)}, f32[4,2]{0,1:T(2,128)}, u32[]{:S(2)}) copy-start(f32[4,2]{0,1:T(2,128)} %copy-done.22) | copy-start | bytes 100
  156.6 52.6 %copy-start.28 = (f32[4,2]{0,1:T(2,128)S(1)}, f32[4,2]{0,1:T(2,128)}, u32[]{:S(2)}) copy-start(f32[4,2]{0,1:T(2,128)} %fusion.116) | copy-start | bytes 100
  156.6 52.6 %copy-start.29 = (f32[4,2]{0,1:T(2,128)S(1)}, f32[4,2]{0,1:T(2,128)}, u32[]{:S(2)}) copy-start(f32[4,2]{0,1:T(2,128)} %exp.97) | copy-start | bytes 100
  156.6 52.6 %copy-start.33 = (pred[4,4]{1,0:T(4,128)(4,1)S(1)}, pred[4,4]{1,0:T(4,128)(4,1)}, u32[]{:S(2)}) copy-start(pred[4,4]{1,0:T(4,128)(4,1)} %iota_compare_fusion.1) | copy-start | bytes 52
  158.4 51.1 %copy-start.4 = (bf16[4,128,128,1]{2,1,3,0:T(8,128)(2,1)S(1)}, bf16[4,128,128,1]{2,1,3,0:T(8,128)(2,1)}, u32[]{:S(2)}) copy-start(bf16[4,128,128,1]{2,1,3,0:T(8,128)(2,1)} %copy.198) | copy-start | bytes 393220
  158.7 51.0 %copy-start.20 = (f32[16,1,2]{0,2,1:T(2,128)S(1)}, f32[16,1,2]{0,2,1:T(2,128)}, u32[]{:S(2)}) copy-start(f32[16,1,2]{0,2,1:T(2,128)} %copy.178) | copy-start | bytes 388
  159.1 51.0 %copy-start.30 = (f32[4,2]{0,1:T(2,128)S(1)}, f32[4,2]{0,1:T(2,128)}, u32[]{:S(2)}) copy-start(f32[4,2]{0,1:T(2,128)} %get-tuple-element.12) | copy-start | bytes 100
  159.1 51.0 %copy-start.32 = (pred[4,4]{1,0:T(4,128)(4,1)S(1)}, pred[4,4]{1,0:T(4,128)(4,1)}, u32[]{:S(2)}) copy-start(pred[4,4]{1,0:T(4,128)(4,1)} %iota_compare_fusion) | copy-start | bytes 52
  185.6 25.1 %copy-start.11 = (bf16[16,4,8,128]{3,2,1,0:T(8,128)(2,1)S(1)}, bf16[16,4,8,128]{3,2,1,0:T(8,128)(2,1)}, u32[]{:S(2)}) copy-start(bf16[16,4,8,128]{3,2,1,0:T(8,128)(2,1)} %get-tuple-element.16) | copy-start | bytes 393220
  185.6 25.1 %copy-start.12 = (bf16[16,4,8,128]{3,2,1,0:T(8,128)(2,1)S(1)}, bf16[16,4,8,128]{3,2,1,0:T(8,128)(2,1)}, u32[]{:S(2)}) copy-start(bf16[16,4,8,128]{3,2,1,0:T(8,128)(2,1)} %get-tuple-element.17) | copy-start | bytes 393220
  211.5 2.0 copy-start.31
  213.4 1.5 copy-start.10
  213.5 1.5 copy-start.15
  213.5 1.5 copy-start.17
  214.7 0.7 copy-start.24
  214.9 0.9 copy-start.16
Sparse Core Ops, SparseCore 0:
  15.6 102.1 all-gather.4
where the time goes:
time: 285 us; the launch traced here: 283 us
  blocking collectives  134 us (47%)
  waiting for transfers between devices  53.6 us (19%)
  local copies, waits for them, and re-layouts  24.2 us (8%)
  matrix products  24.1 us (8%)
  other arithmetic  21.7 us (8%)
  between operations  14.9 us (5%)
  starting transfers between devices  10.5 us (4%)
    all_to_all x1, blocking collectives, summed_on_arrival(): lax.all_to_all(pieces, axis, split_axis=0, concat_axis=0, tiled=True)  54.8 us
    all_gather x1, waiting for transfers between devices, turned_gather(): out = lax.all_gather(both, axis, axis=0, tiled=True)  52.4 us
    unnamed x1, blocking collectives  31.4 us
    all_gather x1, blocking collectives, shards(): lax.all_gather(summary_fwd[None].astype(jnp.bfloat16), 'sp', axis=0, tile...  24.8 us
    all_gather x1, blocking collectives, shards(): lax.all_gather(summary_bwd[None].astype(jnp.bfloat16), 'sp', axis=0, tile...  23.2 us
    dot_general x7, matrix products, shards(): jnp.dot(normed, matrix, preferred_element_type=jnp.float32)  13.4 us
    unnamed x88, local copies, waits for them, and re-layouts  11.8 us
    ppermute x2, starting transfers between devices, extended(): lax.ppermute(tail, axis, [(i, (i + 1) % count) for i in range(ends)])  7.72 us
  transfers between devices with their start and end apart: 5, of which 2 were waited for; matrix products, arithmetic and copies ran while one was open for 16% of the time, Pallas kernels for 0%

commit v1 on v0

v1 whole, which is shorter than its diff:
```python
import functools

import jax
import jax.numpy as jnp
from jax import lax
from jax.experimental import pallas as pl
from jax.experimental.pallas import tpu as pltpu
from jax.sharding import PartitionSpec as P

BLOCK = 128
LANES = 128
HALO = 16
GRID_WIDTH = 64
QUARTER = 32
WIN_COLS = 1024
F32 = jnp.float32
BF16 = jnp.bfloat16
HIGHEST = lax.Precision.HIGHEST


def modulo(value, count):
    return lax.rem(value + 2 * count, count)


def half_lanes(shape):
    return lax.broadcasted_iota(jnp.int32, shape, 1) < LANES // 2


def dot(a, b, precision=None):
    return jnp.dot(a, b, preferred_element_type=F32, precision=precision)


def kernel(
    n,
    ny,
    nx,
    tokens,
    norm_gain,
    gate_w,
    value_w,
    keys_w,
    query_w,
    step_w,
    rate,
    jumps,
    gain,
    filter_value,
    filter_keys,
    filter_query,
    wq_w,
    wk_w,
    wv_w,
    sink,
    out_state_w,
    out_window_w,
    result,
    win,
    wout,
    normed,
    acc,
    halo_in,
    pre,
    cos_t,
    sin_t,
    step_b,
    cum_b,
    step_cols,
    scan_v,
    scan_k,
    scan_q,
    query_rot,
    kv_ext,
    state_a,
    state_c,
    carry_f,
    carry_b,
    scan_loc,
    message,
    arrived,
    totals_out,
    totals,
    incoming,
    income_out,
    mix,
    pair_out,
    pair_in,
    own_part,
    group_out,
    group_in,
    load_sem,
    zs,
    zr,
    ys,
    yr,
    hs,
    hr,
    ks,
    kr,
    a1s,
    a1r,
    a2s,
    a2r,
    ts,
    tr,
    ps,
    pr,
    gs,
    gr,
):
    rows = tokens.shape[0]
    blocks = rows // BLOCK
    depth = tokens.shape[1]
    shard = depth // n
    me = lax.axis_index("sp")
    my_y = lax.axis_index("fs")
    my_tp = lax.axis_index("tp")
    core = lax.rem(my_tp, 2)
    my_x = my_tp // 2
    right, left = modulo(me + 1, n), modulo(me - 1, n)
    up, down = modulo(my_y + 1, ny), modulo(my_y - 1, ny)
    partner = my_tp + 1 - 2 * core
    own_half = lax.rem(my_y, 2)
    half = n // 2

    loads = []
    column = 0
    for k, ref in enumerate((value_w, keys_w, query_w, gate_w, wq_w, wk_w, wv_w)):
        width = ref.shape[1]
        loads.append(
            pltpu.make_async_copy(
                ref, win.at[me, :, pl.ds(column, width)], load_sem.at[k]
            )
        )
        column += width
    loads.append(
        pltpu.make_async_copy(out_state_w, wout.at[me, pl.ds(0, LANES), :], load_sem.at[7])
    )
    loads.append(
        pltpu.make_async_copy(
            out_window_w, wout.at[me, pl.ds(LANES, 2 * LANES), :], load_sem.at[8]
        )
    )
    for load in loads:
        load.start()

    barrier = pltpu.get_barrier_semaphore()
    peers = [{"sp": modulo(me + o, n)} for o in range(1, n)]
    peers += [{"fs": modulo(my_y + o, ny)} for o in sorted({1, ny - 1})]
    peers += [{"tp": partner}]
    peers += [{"tp": 2 * modulo(my_x + o, nx) + core} for o in range(1, nx)]
    for peer in peers:
        pl.semaphore_signal(barrier, inc=1, device_id=peer)
    for load in loads:
        load.wait()
    pl.semaphore_wait(barrier, len(peers))

    def halo_copy(d):
        source = tokens.at[pl.ds(rows - HALO, HALO)] if d == 0 else tokens.at[pl.ds(0, HALO)]
        return pltpu.make_async_remote_copy(
            source,
            halo_in.at[d],
            hs.at[d],
            hr.at[d],
            device_id={"sp": right if d == 0 else left},
        )

    buffers = (win, wout)

    def part(k, source, which, q):
        size = buffers[k].shape[1] // 4
        start = pl.multiple_of((2 * which + q) * size, size)
        return buffers[k].at[source, pl.ds(start, size)]

    def origin(d, s):
        return modulo(me - s, n) if d == 0 else modulo(me + s, n)

    def z_copy(d, s, k, q):
        ref = part(k, origin(d, s - 1), own_half, q)
        return pltpu.make_async_remote_copy(
            ref,
            ref,
            zs.at[d, s - 1, 2 * k + q],
            zr.at[d, s - 1, 2 * k + q],
            device_id={"sp": right if d == 0 else left},
        )

    def z_arrival(d, s, k, q):
        ref = part(k, origin(d, s), own_half, q)
        return pltpu.make_async_remote_copy(
            ref,
            ref,
            zs.at[d, s - 1, 2 * k + q],
            zr.at[d, s - 1, 2 * k + q],
            device_id={"sp": right if d == 0 else left},
        )

    def y_copy(d, s, k, q, which):
        ref = part(k, origin(d, s), which, q)
        return pltpu.make_async_remote_copy(
            ref,
            ref,
            ys.at[d, s - 1, 2 * k + q],
            yr.at[d, s - 1, 2 * k + q],
            device_id={"fs": up if q == 0 else down},
        )

    for d in range(2):
        halo_copy(d).start()
    for k in range(2):
        for q in range(2):
            for d in range(2):
                if half > 1 or q == d:
                    z_copy(d, 1, k, q).start()

    def normalise(x):
        wide = x.astype(F32)
        scale = lax.rsqrt(jnp.mean(wide * wide, axis=-1, keepdims=True) + 1e-06)
        return (wide * scale * norm_gain[...]).astype(BF16)

    def normalise_chunk(i, carry):
        start = pl.multiple_of(i * 32, 32)
        normed[pl.ds(HALO + start, 32), :] = normalise(tokens[pl.ds(start, 32), :])
        return carry

    lax.fori_loop(0, rows // 32, normalise_chunk, 0)
    for d in range(2):
        halo_copy(d).wait_recv()
        normed[(0 if d == 0 else HALO + rows) : (HALO if d == 0 else 2 * HALO + rows), :] = (
            normalise(halo_in[d])
        )

    def project(source, first):
        x = normed[:, pl.ds(pl.multiple_of(source * shard, shard), shard)]
        for c in range(0, WIN_COLS, 256):
            term = dot(x, win[source, :, c : c + 256])
            if first:
                acc[:, c : c + 256] = term
            else:
                acc[:, c : c + 256] += term

    project(me, True)

    heads = lax.broadcasted_iota(jnp.int32, (step_w.shape[1], LANES), 0)
    lanes_of = lax.broadcasted_iota(jnp.int32, (step_w.shape[1], LANES), 1)
    spread = (heads == 2 * my_tp + lanes_of // (LANES // 2)).astype(BF16)
    step_cols[...] = dot(step_w[...], spread).astype(BF16)
    tri = (
        lax.broadcasted_iota(jnp.int32, (BLOCK, BLOCK), 0)
        >= lax.broadcasted_iota(jnp.int32, (BLOCK, BLOCK), 1)
    ).astype(F32)
    first_head = half_lanes((1, LANES))

    def decay_block(b):
        start = pl.multiple_of(b * BLOCK, BLOCK)
        raw = dot(normed[pl.ds(HALO + start, BLOCK), :], step_cols[...])
        step = jnp.maximum(raw, 0.0) + jnp.log1p(jnp.exp(-jnp.abs(raw)))
        rate_row = jnp.where(first_head, rate[0], rate[1])
        jump = jumps[pl.ds(start, BLOCK), :]
        logs = -rate_row * step + jnp.where(first_head, jump[:, 0:1], jump[:, 1:2])
        step_b[pl.ds(start, BLOCK), :] = step
        cum_b[pl.ds(start, BLOCK), :] = dot(tri, logs, HIGHEST)

    angle_rows = rows // half

    def angle_block(i):
        start = pl.multiple_of(i * angle_rows, angle_rows)
        lane = lax.broadcasted_iota(jnp.int32, (angle_rows, LANES), 1)
        position = (
            lax.broadcasted_iota(jnp.int32, (angle_rows, LANES), 0) + me * rows + start
        )
        row_at = (position // GRID_WIDTH).astype(F32)
        col_at = lax.rem(position, GRID_WIDTH).astype(F32)
        exponent = lax.rem(lane, QUARTER).astype(F32) / -QUARTER
        inverse = jnp.exp(exponent[0:8] * 9.210340371976184)[0:1]
        angle = jnp.where(lane < LANES // 2, row_at, col_at) * inverse
        sine = jnp.sin(angle)
        cos_t[pl.ds(start, angle_rows), :] = jnp.cos(angle)
        sin_t[pl.ds(start, angle_rows), :] = jnp.where(
            lax.rem(lane, 2 * QUARTER) < QUARTER, -sine, sine
        )

    other_half = 1 - own_half

    def gather_step(s, carry):
        @pl.when(s < half)
        def _():
            for k in range(2):
                for q in range(2):
                    for d in range(2):
                        z_arrival(d, s, k, q).wait_recv()
                        if q == d:
                            z_copy(d, s + 1, k, q).start()
                        else:

                            @pl.when(s + 1 < half)
                            def _():
                                z_copy(d, s + 1, k, q).start()

                        y_copy(d, s, k, q, own_half).start()

        @pl.when(s == half)
        def _():
            for k in range(2):
                for d in range(2):
                    z_arrival(d, s, k, d).wait_recv()
                    y_copy(d, s, k, d, own_half).start()

        @pl.when(s <= half)
        def _():
            angle_block(s - 1)

        @pl.when(s <= blocks)
        def _():
            decay_block(s - 1)

        before = s - 1

        @pl.when((before >= 1) & (before < half))
        def _():
            for d in range(2):
                for q in range(2):
                    y_copy(d, before, 0, q, other_half).wait_recv()
            for d in range(2):
                project(origin(d, before), False)

        @pl.when(before == half)
        def _():
            for d in range(2):
                y_copy(d, before, 0, d, other_half).wait_recv()
            project(origin(0, before), False)

        return carry

    lax.fori_loop(1, half + 2, gather_step, 0)
    for b in range(half, blocks):
        if b > half:
            decay_block(b)

    def rotate(x, b):
        start = pl.multiple_of(b * BLOCK, BLOCK)
        wide = x.astype(BF16).astype(F32)
        lane = lax.broadcasted_iota(jnp.int32, (BLOCK, LANES), 1)
        turned = jnp.where(
            lax.rem(lane, 2 * QUARTER) < QUARTER,
            pltpu.roll(wide, LANES - QUARTER, 1),
            pltpu.roll(wide, QUARTER, 1),
        )
        return (
            wide * cos_t[pl.ds(start, BLOCK), :] + turned * sin_t[pl.ds(start, BLOCK), :]
        ).astype(BF16)

    def key_block(b, carry):
        start = pl.multiple_of(b * BLOCK, BLOCK)
        own = pl.ds(HALO + start, BLOCK)
        target = pl.ds(BLOCK + start, BLOCK)
        kv_ext[target, 0:LANES] = rotate(acc[own, 768:896], b)
        kv_ext[target, LANES : 2 * LANES] = acc[own, 896:1024].astype(BF16)
        return carry

    def query_block(b, carry):
        start = pl.multiple_of(b * BLOCK, BLOCK)
        own = pl.ds(HALO + start, BLOCK)
        for h in range(2):
            query_rot[pl.ds(start, BLOCK), h * LANES : (h + 1) * LANES] = rotate(
                acc[own, 512 + h * LANES : 512 + (h + 1) * LANES], b
            )
        return carry

    lax.fori_loop(0, blocks, key_block, 0)

    def kv_copy(d):
        source = kv_ext.at[pl.ds(rows if d == 0 else BLOCK, BLOCK)]
        return pltpu.make_async_remote_copy(
            source,
            kv_ext.at[pl.ds(0 if d == 0 else rows + BLOCK, BLOCK)],
            ks.at[d],
            kr.at[d],
            device_id={"sp": right if d == 0 else left},
        )

    pre[...] = acc[:, 0:384].astype(BF16).astype(F32)

    @pl.when(me == 0)
    def _():
        pre[0:HALO, :] = jnp.zeros((HALO, 384), F32)

    @pl.when(me == n - 1)
    def _():
        pre[HALO + rows : 2 * HALO + rows, :] = jnp.zeros((HALO, 384), F32)

    for d in range(2):
        kv_copy(d).start()

    taps = [f[...].astype(F32) for f in (filter_value, filter_keys, filter_query)]
    for b in range(blocks):
        for c in range(3):
            total = jnp.zeros((BLOCK, LANES), F32)
            for j in range(5):
                at = HALO + b * BLOCK + j - 2
                total = total + (
                    pre[at : at + BLOCK, c * LANES : (c + 1) * LANES] * taps[c][j : j + 1, :]
                )
            here = slice(b * BLOCK, (b + 1) * BLOCK)
            if c == 0:
                scan_v[here, :] = total * jax.nn.sigmoid(total) * step_b[here, :]
            elif c == 1:
                scan_k[here, :] = total.astype(BF16)
            else:
                scan_q[here, :] = total.astype(BF16)

    def block_states(b, carry):
        start = pl.multiple_of(b * BLOCK, BLOCK)
        here = pl.ds(start, BLOCK)
        cum = cum_b[here, :]
        total = cum[BLOCK - 1 : BLOCK, :]
        values = scan_v[here, :].astype(BF16).astype(F32)
        keys_t = scan_k[here, :].astype(F32).T.astype(BF16)
        state_a[b] = dot(keys_t, (values * jnp.exp(total - cum)).astype(BF16))
        state_c[b] = dot(keys_t, (values * jnp.exp(cum)).astype(BF16))
        return carry

    lax.fori_loop(0, blocks, block_states, 0)
    ends = [cum_b[(b + 1) * BLOCK - 1 : (b + 1) * BLOCK, :] for b in range(blocks)]
    forward = jnp.zeros((BLOCK, LANES), F32)
    for b in range(blocks):
        carry_f[b] = forward.astype(BF16)
        forward = forward * jnp.exp(ends[b]) + state_a[b]
    backward = jnp.zeros((BLOCK, LANES), F32)
    for b in reversed(range(blocks)):
        carry_b[b] = backward.astype(BF16)
        backward = backward * jnp.exp(ends[b]) + state_c[b]
    overall = functools.reduce(jnp.add, ends)

    piece = BLOCK // n
    message[...] = jnp.concatenate(
        [forward.reshape(n, piece, LANES), backward.reshape(n, piece, LANES)], axis=1
    ).astype(BF16)
    totals_out[...] = overall
    totals[me] = overall
    arrived[me] = message[me]

    def first_exchange(o):
        to = modulo(me + o, n)
        return (
            pltpu.make_async_remote_copy(
                message.at[to], arrived.at[me], a1s.at[o], a1r.at[o], device_id={"sp": to}
            ),
            pltpu.make_async_remote_copy(
                totals_out, totals.at[me], ts.at[o], tr.at[o], device_id={"sp": to}
            ),
        )

    def first_arrival(o):
        source = modulo(me - o, n)
        return (
            pltpu.make_async_remote_copy(
                arrived.at[source], arrived.at[source], a1s.at[o], a1r.at[o], device_id={"sp": source}
            ),
            pltpu.make_async_remote_copy(
                totals.at[source], totals.at[source], ts.at[o], tr.at[o], device_id={"sp": source}
            ),
        )

    order = sorted(range(1, n), key=lambda o: -min(o, n - o))
    for o in order:
        for copy in first_exchange(o):
            copy.start()

    near_mask = half_lanes((BLOCK, LANES))

    def local_scan(b, carry):
        start = pl.multiple_of(b * BLOCK, BLOCK)
        here = pl.ds(start, BLOCK)
        cum = cum_b[here, :]
        cum_t = cum.T
        total = cum[BLOCK - 1 : BLOCK, :]
        values = scan_v[here, :].astype(BF16)
        query = scan_q[here, :]
        gram = lax.dot_general(
            query, scan_k[here, :], (((1,), (1,)), ((), ())), preferred_element_type=F32
        )
        near = []
        for h in range(2):
            lane = h * (LANES // 2)
            gap = jnp.abs(cum[:, lane : lane + 1] - cum_t[lane : lane + 1, :])
            near.append(dot((gram * jnp.exp(-gap)).astype(BF16), values))
        out = jnp.where(near_mask, near[0], near[1])
        out += jnp.exp(cum) * dot(query, carry_f[b])
        out += jnp.exp(total - cum) * dot(query, carry_b[b])
        scan_loc[here, :] = out
        return carry

    lax.fori_loop(0, blocks, local_scan, 0)

    for o in order:
        for copy in first_arrival(o):
            copy.wait_recv()

    running = jnp.zeros((piece, LANES), F32)
    ahead = []
    for d in range(n):
        ahead.append(running)
        running = running * jnp.exp(totals[d]) + arrived[d].astype(F32)[0:piece]
    running = jnp.zeros((piece, LANES), F32)
    behind = [None] * n
    for d in reversed(range(n)):
        behind[d] = running
        running = running * jnp.exp(totals[d]) + arrived[d].astype(F32)[piece : 2 * piece]
    for d in range(n):
        income_out[d] = jnp.concatenate([ahead[d], behind[d]], axis=0).astype(BF16)
    incoming[me] = income_out[me]

    def second_exchange(o):
        to = modulo(me + o, n)
        return pltpu.make_async_remote_copy(
            income_out.at[to], incoming.at[me], a2s.at[o], a2r.at[o], device_id={"sp": to}
        )

    def second_arrival(o):
        source = modulo(me - o, n)
        return pltpu.make_async_remote_copy(
            incoming.at[source], incoming.at[source], a2s.at[o], a2r.at[o], device_id={"sp": source}
        )

    for o in order:
        second_exchange(o).start()

    lax.fori_loop(0, blocks, query_block, 0)
    for d in range(2):
        kv_copy(d).wait_recv()

    def attend(b, carry):
        start = pl.multiple_of(b * BLOCK, BLOCK)
        band = kv_ext[pl.ds(start, 3 * BLOCK), :]
        row = lax.broadcasted_iota(jnp.int32, (BLOCK, 3 * BLOCK), 0)
        col = lax.broadcasted_iota(jnp.int32, (BLOCK, 3 * BLOCK), 1)
        where_key = me * rows - BLOCK + start + col
        valid = (
            (jnp.abs(col - BLOCK - row) <= BLOCK) & (where_key >= 0) & (where_key < n * rows)
        )
        for h in range(2):
            query = query_rot[pl.ds(start, BLOCK), h * LANES : (h + 1) * LANES]
            scores = lax.dot_general(
                query, band[:, 0:LANES], (((1,), (1,)), ((), ())), preferred_element_type=F32
            ) * LANES ** (-0.5)
            masked = jnp.where(valid, scores, -1e30)
            ceiling = jnp.maximum(jnp.max(masked, axis=-1, keepdims=True), sink[h])
            weights = jnp.where(valid, jnp.exp(masked - ceiling), 0.0)
            bottom = jnp.exp(sink[h] - ceiling) + jnp.sum(weights, axis=-1, keepdims=True)
            probs = (weights / bottom).astype(BF16)
            mix[pl.ds(start, BLOCK), (1 + h) * LANES : (2 + h) * LANES] = dot(
                probs, band[:, LANES : 2 * LANES]
            ).astype(BF16)
        return carry

    lax.fori_loop(0, blocks, attend, 0)

    for o in order:
        second_arrival(o).wait_recv()
    incomes = incoming[...].astype(F32)
    income_f = incomes[:, 0:piece].reshape(BLOCK, LANES).astype(BF16)
    income_b = incomes[:, piece : 2 * piece].reshape(BLOCK, LANES).astype(BF16)
    befores = [jnp.zeros((1, LANES), F32)]
    for b in range(blocks):
        befores.append(befores[-1] + ends[b])
    for b in range(blocks):
        here = slice(b * BLOCK, (b + 1) * BLOCK)
        cum = cum_b[here, :]
        query = scan_q[here, :]
        after = overall - befores[b + 1]
        out = scan_loc[here, :]
        out += jnp.exp(cum + befores[b]) * dot(query, income_f)
        out += jnp.exp(ends[b] - cum + after) * dot(query, income_b)
        gate = acc[HALO + b * BLOCK : HALO + (b + 1) * BLOCK, 384:512].astype(BF16).astype(F32)
        gated = out * (gate * jax.nn.sigmoid(gate))
        square = gated * gated
        low = jnp.sum(jnp.where(near_mask, square, 0.0), axis=-1, keepdims=True)
        high = jnp.sum(jnp.where(near_mask, 0.0, square), axis=-1, keepdims=True)
        mean = jnp.where(near_mask, low, high) * (2.0 / LANES)
        mix[here, 0:LANES] = (gated * lax.rsqrt(mean + 1e-06) * gain[...]).astype(BF16)

    def wait_out(s, carry):
        @pl.when(s < half)
        def _():
            for d in range(2):
                for q in range(2):
                    y_copy(d, s, 1, q, other_half).wait_recv()

        @pl.when(s == half)
        def _():
            for d in range(2):
                y_copy(d, s, 1, d, other_half).wait_recv()

        return carry

    lax.fori_loop(1, half + 1, wait_out, 0)
    unit = rows // (2 * nx)

    def rows_for(c):
        return jnp.concatenate(
            [
                mix[pl.ds(pl.multiple_of((2 * x + c) * unit, unit), unit), :]
                for x in range(nx)
            ],
            axis=0,
        )

    def product(lhs, i):
        weights = jnp.concatenate([wout[2 * i], wout[2 * i + 1]], axis=1)
        return dot(lhs, weights).reshape(nx, unit, 2 * LANES)

    def other_product(i, carry):
        columns = pl.ds(pl.multiple_of(i * 2 * LANES, 2 * LANES), 2 * LANES)
        pair_out[:, :, columns] = product(rows_for(1 - core), i).astype(BF16)
        return carry

    def own_product(i, carry):
        columns = pl.ds(pl.multiple_of(i * 2 * LANES, 2 * LANES), 2 * LANES)
        own_part[:, :, columns] = product(rows_for(core), i)
        return carry

    def pair_copy(x):
        return pltpu.make_async_remote_copy(
            pair_out.at[x], pair_in.at[x], ps.at[x], pr.at[x], device_id={"tp": partner}
        )

    lax.fori_loop(0, n // 2, other_product, 0)
    for x in range(nx):
        pair_copy(x).start()
    lax.fori_loop(0, n // 2, own_product, 0)
    for x in range(nx):
        pair_copy(x).wait_recv()

    def group_copy(o):
        to = modulo(my_x + o, nx)
        return pltpu.make_async_remote_copy(
            group_out.at[o - 1],
            group_in.at[o - 1],
            gs.at[o - 1],
            gr.at[o - 1],
            device_id={"tp": 2 * to + core},
        )

    def group_sum(o):
        to = modulo(my_x + o, nx)
        return own_part[to] + pair_in[to].astype(F32)

    x_order = sorted(range(1, nx), key=lambda o: -min(o, nx - o))
    for o in x_order:
        group_out[o - 1] = group_sum(o).astype(BF16)
        group_copy(o).start()
    mine = group_sum(0)
    for o in x_order:
        group_copy(o).wait_recv()
        mine = mine + group_in[o - 1].astype(F32)
    result[...] = mine.astype(BF16)

    for d in range(2):
        halo_copy(d).wait_send()
        kv_copy(d).wait_send()
    for o in order:
        for copy in first_exchange(o):
            copy.wait_send()
        second_exchange(o).wait_send()
    for x in range(nx):
        pair_copy(x).wait_send()
    for o in x_order:
        group_copy(o).wait_send()

    def drain(s, carry):
        for k in range(2):
            for q in range(2):
                for d in range(2):
                    if q == d:
                        z_copy(d, s, k, q).wait_send()
                        y_copy(d, s, k, q, own_half).wait_send()
                    else:

                        @pl.when(s < half)
                        def _():
                            z_copy(d, s, k, q).wait_send()
                            y_copy(d, s, k, q, own_half).wait_send()

        return carry

    lax.fori_loop(1, half + 1, drain, 0)


def solution(mesh):
    n, ny, nt = (mesh.shape[a] for a in ("sp", "fs", "tp"))
    nx = nt // 2

    def shards(*args):
        args = list(args)
        rows, depth = args[0].shape
        args[1] = args[1].reshape(1, -1)
        args[9] = args[9].reshape(1, -1)
        shard = depth // n
        half = n // 2
        blocks = rows // BLOCK
        piece = BLOCK // n
        unit = rows // (2 * nx)
        vmem = pl.BlockSpec(memory_space=pltpu.VMEM)
        smem = pl.BlockSpec(memory_space=pltpu.SMEM)
        anywhere = pl.BlockSpec(memory_space=pl.ANY)
        specs = [vmem] * 19
        specs[7] = specs[16] = smem
        for i in (2, 3, 4, 5, 13, 14, 15, 17, 18):
            specs[i] = anywhere
        dma = pltpu.SemaphoreType.DMA
        V = pltpu.VMEM
        scratch = [
            V((n, shard, WIN_COLS), BF16),
            V((n, 3 * LANES, LANES), BF16),
            V((rows + 2 * HALO, depth), BF16),
            V((rows + 2 * HALO, WIN_COLS), F32),
            V((2, HALO, depth), BF16),
            V((rows + 2 * HALO, 3 * LANES), F32),
            V((rows, LANES), F32),
            V((rows, LANES), F32),
            V((rows, LANES), F32),
            V((rows, LANES), F32),
            V((depth, LANES), BF16),
            V((rows, LANES), F32),
            V((rows, LANES), BF16),
            V((rows, LANES), BF16),
            V((rows, 2 * LANES), BF16),
            V((rows + 2 * BLOCK, 2 * LANES), BF16),
            V((blocks, BLOCK, LANES), F32),
            V((blocks, BLOCK, LANES), F32),
            V((blocks, BLOCK, LANES), BF16),
            V((blocks, BLOCK, LANES), BF16),
            V((rows, LANES), F32),
            V((n, 2 * piece, LANES), BF16),
            V((n, 2 * piece, LANES), BF16),
            V((1, LANES), F32),
            V((n, 1, LANES), F32),
            V((n, 2 * piece, LANES), BF16),
            V((n, 2 * piece, LANES), BF16),
            V((rows, 3 * LANES), BF16),
            V((nx, unit, depth), BF16),
            V((nx, unit, depth), BF16),
            V((nx, unit, depth), F32),
            V((max(nx - 1, 1), unit, depth), BF16),
            V((max(nx - 1, 1), unit, depth), BF16),
            dma((9,)),
            dma((2, half, 4)),
            dma((2, half, 4)),
            dma((2, half, 4)),
            dma((2, half, 4)),
            dma((2,)),
            dma((2,)),
            dma((2,)),
            dma((2,)),
            dma((n,)),
            dma((n,)),
            dma((n,)),
            dma((n,)),
            dma((n,)),
            dma((n,)),
            dma((nx,)),
            dma((nx,)),
            dma((max(nx - 1, 1),)),
            dma((max(nx - 1, 1),)),
        ]
        return pl.pallas_call(
            functools.partial(kernel, n, ny, nx),
            out_shape=jax.ShapeDtypeStruct((rows // nt, depth), BF16),
            in_specs=specs,
            out_specs=vmem,
            scratch_shapes=scratch,
            compiler_params=pltpu.CompilerParams(
                collective_id=0, has_side_effects=True, vmem_limit_bytes=60 * 1024 * 1024
            ),
        )(*args)

    placed = (
        P(("fs", "sp"), None),
        P(),
        P("sp", "tp"),
        P("sp", "tp"),
        P("sp", "tp"),
        P("sp", "tp"),
        P(),
        P("tp"),
        P(("fs", "sp"), "tp"),
        P("tp"),
        P(None, "tp"),
        P(None, "tp"),
        P(None, "tp"),
        P("sp", "tp"),
        P("sp", "tp"),
        P("sp", "tp"),
        P("tp"),
        P("tp", "sp"),
        P("tp", "sp"),
    )
    return jax.shard_map(
        shards, mesh=mesh, in_specs=placed, out_specs=P(("fs", "sp", "tp"), None), check_vma=False
    )
```

time: 285 us -> 103 us (0.36)
  blocking collectives: 134 us -> 0 us
  Pallas kernels: 0 us -> 97.6 us
  waiting for transfers between devices: 53.6 us -> 0 us
  matrix products: 24.1 us -> 0 us
  other arithmetic: 21.7 us -> 0 us
  local copies, waits for them, and re-layouts: 24.2 us -> 5.05 us
  between operations: 14.9 us -> 0.01 us
  starting transfers between devices: 10.5 us -> 0 us
    pallas_call x0 -> x1, Pallas kernels: none -> 97.6 us  [shards(): pl.pallas_call(functools.partial(kernel, n, ny, nx), out_shape=jax.ShapeD...]
    all_to_all x1 -> x0, blocking collectives: 54.8 us -> none  [summed_on_arrival(): lax.all_to_all(pieces, axis, split_axis=0, concat_axis=0, tiled=True)]
    all_gather x1 -> x0, waiting for transfers between devices: 52.4 us -> none  [turned_gather(): out = lax.all_gather(both, axis, axis=0, tiled=True)]
    all_gather x2 -> x0, blocking collectives: 48 us -> none  [the longest x1 24.8 us: shards(): lax.all_gather(summary_fwd[None].astype(jnp.bfloat16), 'sp', axis=0, tile...]
    unnamed x1 -> x0, blocking collectives: 31.4 us -> none
    dot_general x24 -> x0, matrix products: 24.1 us -> none  [the longest x7 13.4 us: shards(): jnp.dot(normed, matrix, preferred_element_type=jnp.float32)]
    ppermute x4 -> x0, starting transfers between devices: 10.5 us -> none  [the longest x2 7.72 us: extended(): lax.ppermute(tail, axis, [(i, (i + 1) % count) for i in range(ends)])]
    unnamed x88 -> x3, local copies, waits for them, and re-layouts: 11.8 us -> 5.05 us
  transfers between devices with their start and end apart: 5 -> 0, of which waited for: 2 -> 0; matrix products, arithmetic and copies ran while one was open for 16% -> 0% of each run, Pallas kernels for 0% -> 0%
where the time goes in v1:
time: 103 us
  Pallas kernels  97.6 us (95%)
  local copies, waits for them, and re-layouts  5.05 us (5%)
    pallas_call x1, Pallas kernels, shards(): pl.pallas_call(functools.partial(kernel, n, ny, nx), out_shape=jax.ShapeD...  97.6 us
    unnamed x3, local copies, waits for them, and re-layouts  5.05 us

profile of v1, /device:TPU:1, one launch (start us, length us, event | category | flops | bytes accessed | tf_op | source)
XLA Modules:
  0.0 102.6 jit_solution(14941545271588647054)
XLA Ops:
  0.0 1.5 %copy.21.jumps = f32[512,2]{1,0:T(8,128)} copy(f32[512,2]{0,1:T(2,128)} %param.27) | data formatting | bytes 8192 | tf_op args[8]
  1.5 1.8 %copy.20.step_w = bf16[2048,16]{1,0:T(8,128)(2,1)} copy(bf16[2048,16]{0,1:T(8,128)(2,1)} %param.25) | data formatting | bytes 131072 | tf_op args[6]
  3.4 97.6 %shard_map.181 = bf16[64,2048]{1,0:T(8,128)(2,1)} custom-call(bf16[512,2048]{1,0:T(8,128)(2,1)} %tokens.1, f32[1,2048]{1,0:T(1,128)} %bitcast.2, bf16[128,128]{1,0:T(8,128)(2,1)} %gate_w.1, bf16[128,128]{1,0:T(8,128)(2,1)} %value_w.1, bf16[128,128]{1,0:T(8,128)(2,1)} %keys_w.1, bf16[128,128]{1,0:T(8,128)(2,1)} %query_w.1, bf16[2048,16]{1,0:T(8,128)(2,1)} %copy.20.step_w, ...), custom_call_target="tpu_custom_call" | custom-call | tf_op jit(solution)/shard_map/pallas_call | solution.py:766
  101.0 1.7 %copy.23 = bf16[64,2048]{1,0:T(8,128)(2,1)} copy(bf16[64,2048]{1,0:T(8,128)(2,1)} %shard_map.181) | data formatting | bytes 524288

commit v2 on v1

--- a/solution.py
+++ b/solution.py
@@ -13,6 +13,8 @@
 GRID_WIDTH = 64
 QUARTER = 32
 WIN_COLS = 1024
+PIECES = 4
+OUT_EARLY = 3
 F32 = jnp.float32
 BF16 = jnp.bfloat16
 HIGHEST = lax.Precision.HIGHEST
@@ -34,12 +36,28 @@
     n,
     ny,
     nx,
-    tokens,
-    norm_gain,
+    tokens_h,
+    norm_gain_h,
     gate_w,
     value_w,
     keys_w,
     query_w,
+    step_h,
+    rate_h,
+    jumps_h,
+    gain_h,
+    filter_value_h,
+    filter_keys_h,
+    filter_query_h,
+    wq_w,
+    wk_w,
+    wv_w,
+    sink_h,
+    out_state_w,
+    out_window_w,
+    result,
+    tokens,
+    norm_gain,
     step_w,
     rate,
     jumps,
@@ -47,13 +65,7 @@
     filter_value,
     filter_keys,
     filter_query,
-    wq_w,
-    wk_w,
-    wv_w,
     sink,
-    out_state_w,
-    out_window_w,
-    result,
     win,
     wout,
     normed,
@@ -82,16 +94,24 @@
     incoming,
     income_out,
     mix,
+    part_sum,
     pair_out,
     pair_in,
-    own_part,
-    group_out,
-    group_in,
+    via_out,
+    via_in,
+    direct_out,
+    direct_in,
+    merged_out,
+    merged_in,
     load_sem,
     zs,
     zr,
     ys,
     yr,
+    czs,
+    czr,
+    cys,
+    cyr,
     hs,
     hr,
     ks,
@@ -127,27 +147,33 @@
     for k, ref in enumerate((value_w, keys_w, query_w, gate_w, wq_w, wk_w, wv_w)):
         width = ref.shape[1]
         loads.append(
-            pltpu.make_async_copy(
-                ref, win.at[me, :, pl.ds(column, width)], load_sem.at[k]
-            )
+            pltpu.make_async_copy(ref, win.at[me, :, pl.ds(column, width)], load_sem.at[k])
         )
         column += width
-    loads.append(
-        pltpu.make_async_copy(out_state_w, wout.at[me, pl.ds(0, LANES), :], load_sem.at[7])
-    )
-    loads.append(
+    late_loads = [
+        pltpu.make_async_copy(tokens_h, tokens, load_sem.at[9]),
+        pltpu.make_async_copy(norm_gain_h, norm_gain, load_sem.at[10]),
+        pltpu.make_async_copy(step_h, step_w, load_sem.at[11]),
+        pltpu.make_async_copy(rate_h, rate, load_sem.at[12]),
+        pltpu.make_async_copy(jumps_h, jumps, load_sem.at[13]),
+        pltpu.make_async_copy(gain_h, gain, load_sem.at[14]),
+        pltpu.make_async_copy(filter_value_h, filter_value, load_sem.at[15]),
+        pltpu.make_async_copy(filter_keys_h, filter_keys, load_sem.at[16]),
+        pltpu.make_async_copy(filter_query_h, filter_query, load_sem.at[17]),
+        pltpu.make_async_copy(sink_h, sink, load_sem.at[18]),
+        pltpu.make_async_copy(out_state_w, wout.at[me, pl.ds(0, LANES), :], load_sem.at[7]),
         pltpu.make_async_copy(
             out_window_w, wout.at[me, pl.ds(LANES, 2 * LANES), :], load_sem.at[8]
-        )
-    )
-    for load in loads:
+        ),
+    ]
+    for load in loads + late_loads:
         load.start()
 
     barrier = pltpu.get_barrier_semaphore()
-    peers = [{"sp": modulo(me + o, n)} for o in range(1, n)]
+    peers = [{"sp": modulo(me + o, n)} for o in sorted({1, n - 1})]
     peers += [{"fs": modulo(my_y + o, ny)} for o in sorted({1, ny - 1})]
     peers += [{"tp": partner}]
-    peers += [{"tp": 2 * modulo(my_x + o, nx) + core} for o in range(1, nx)]
+    peers += [{"tp": 2 * modulo(my_x + o, nx) + core} for o in sorted({1, nx - 1}) if nx > 1]
     for peer in peers:
         pl.semaphore_signal(barrier, inc=1, device_id=peer)
     for load in loads:
@@ -165,52 +191,101 @@
         )
 
     buffers = (win, wout)
-
-    def part(k, source, which, q):
-        size = buffers[k].shape[1] // 4
-        start = pl.multiple_of((2 * which + q) * size, size)
+    pieces = (PIECES, 2)
+    z_sems = ((zs, zr), (czs, czr))
+    y_sems = ((ys, yr), (cys, cyr))
+
+    def slab(k, source, which, q):
+        size = buffers[k].shape[1] // (2 * pieces[k])
+        start = pl.multiple_of((pieces[k] * which + q) * size, size)
         return buffers[k].at[source, pl.ds(start, size)]
+
+    def lower(k, q):
+        return q < pieces[k] // 2
 
     def origin(d, s):
         return modulo(me - s, n) if d == 0 else modulo(me + s, n)
 
-    def z_copy(d, s, k, q):
-        ref = part(k, origin(d, s - 1), own_half, q)
+    def z_move(d, s, k, q, source):
+        ref = slab(k, source, own_half, q)
+        sent, landed = z_sems[k]
         return pltpu.make_async_remote_copy(
             ref,
             ref,
-            zs.at[d, s - 1, 2 * k + q],
-            zr.at[d, s - 1, 2 * k + q],
+            sent.at[d, s - 1, q],
+            landed.at[d, s - 1, q],
             device_id={"sp": right if d == 0 else left},
         )
 
+    def z_copy(d, s, k, q):
+        return z_move(d, s, k, q, origin(d, s - 1))
+
     def z_arrival(d, s, k, q):
-        ref = part(k, origin(d, s), own_half, q)
+        return z_move(d, s, k, q, origin(d, s))
+
+    def y_copy(d, s, k, q, which):
+        ref = slab(k, origin(d, s), which, q)
+        sent, landed = y_sems[k]
         return pltpu.make_async_remote_copy(
             ref,
             ref,
-            zs.at[d, s - 1, 2 * k + q],
-            zr.at[d, s - 1, 2 * k + q],
-            device_id={"sp": right if d == 0 else left},
-        )
-
-    def y_copy(d, s, k, q, which):
-        ref = part(k, origin(d, s), which, q)
-        return pltpu.make_async_remote_copy(
-            ref,
-            ref,
-            ys.at[d, s - 1, 2 * k + q],
-            yr.at[d, s - 1, 2 * k + q],
-            device_id={"fs": up if q == 0 else down},
-        )
-
+            sent.at[d, s - 1, q],
+            landed.at[d, s - 1, q],
+            device_id={"fs": up if lower(k, q) else down},
+        )
+
+    def last_way(k, q, d):
+        return lower(k, q) == (d == 0)
+
+    def set_off(k):
+        for q in range(pieces[k]):
+            for d in range(2):
+                if half > 1 or last_way(k, q, d):
+                    z_copy(d, 1, k, q).start()
+
+    def relay(k, s):
+        @pl.when(s < half)
+        def _():
+            for q in range(pieces[k]):
+                for d in range(2):
+                    z_arrival(d, s, k, q).wait_recv()
+                    if last_way(k, q, d):
+                        z_copy(d, s + 1, k, q).start()
+                    else:
+
+                        @pl.when(s + 1 < half)
+                        def _():
+                            z_copy(d, s + 1, k, q).start()
+
+                    y_copy(d, s, k, q, own_half).start()
+
+        @pl.when(s == half)
+        def _():
+            for q in range(pieces[k]):
+                for d in range(2):
+                    if last_way(k, q, d):
+                        z_arrival(d, s, k, q).wait_recv()
+                        y_copy(d, s, k, q, own_half).start()
+
+    def y_landed(k, s):
+        @pl.when((s >= 1) & (s < half))
+        def _():
+            for q in range(pieces[k]):
+                for d in range(2):
+                    y_copy(d, s, k, q, 1 - own_half).wait_recv()
+
+        @pl.when(s == half)
+        def _():
+            for q in range(pieces[k]):
+                for d in range(2):
+                    if last_way(k, q, d):
+                        y_copy(d, s, k, q, 1 - own_half).wait_recv()
+
+    set_off(0)
+    for load in late_loads:
+        load.wait()
     for d in range(2):
         halo_copy(d).start()
-    for k in range(2):
-        for q in range(2):
-            for d in range(2):
-                if half > 1 or q == d:
-                    z_copy(d, 1, k, q).start()
 
     def normalise(x):
         wide = x.astype(F32)
@@ -222,41 +297,52 @@
         normed[pl.ds(HALO + start, 32), :] = normalise(tokens[pl.ds(start, 32), :])
         return carry
 
-    lax.fori_loop(0, rows // 32, normalise_chunk, 0)
+    lax.fori_loop(0, rows // 64, normalise_chunk, 0)
+    if half > 1:
+        relay(0, 1)
+    lax.fori_loop(rows // 64, rows // 32, normalise_chunk, 0)
     for d in range(2):
         halo_copy(d).wait_recv()
         normed[(0 if d == 0 else HALO + rows) : (HALO if d == 0 else 2 * HALO + rows), :] = (
             normalise(halo_in[d])
         )
 
-    def project(source, first):
-        x = normed[:, pl.ds(pl.multiple_of(source * shard, shard), shard)]
+    def slice_of(source):
+        return normed[:, pl.ds(pl.multiple_of(source * shard, shard), shard)]
+
+    def project(sources, first):
         for c in range(0, WIN_COLS, 256):
-            term = dot(x, win[source, :, c : c + 256])
+            term = functools.reduce(
+                jnp.add, [dot(slice_of(o), win[o, :, c : c + 256]) for o in sources]
+            )
             if first:
                 acc[:, c : c + 256] = term
             else:
                 acc[:, c : c + 256] += term
 
-    project(me, True)
-
-    heads = lax.broadcasted_iota(jnp.int32, (step_w.shape[1], LANES), 0)
-    lanes_of = lax.broadcasted_iota(jnp.int32, (step_w.shape[1], LANES), 1)
+    heads = lax.broadcasted_iota(jnp.int32, (LANES, step_w.shape[0]), 1)
+    lanes_of = lax.broadcasted_iota(jnp.int32, (LANES, step_w.shape[0]), 0)
     spread = (heads == 2 * my_tp + lanes_of // (LANES // 2)).astype(BF16)
-    step_cols[...] = dot(step_w[...], spread).astype(BF16)
+    step_cols[...] = dot(spread, step_w[...]).astype(BF16)
     tri = (
         lax.broadcasted_iota(jnp.int32, (BLOCK, BLOCK), 0)
         >= lax.broadcasted_iota(jnp.int32, (BLOCK, BLOCK), 1)
     ).astype(F32)
     first_head = half_lanes((1, LANES))
+    first_rows = lax.broadcasted_iota(jnp.int32, (LANES, BLOCK), 0) < LANES // 2
 
     def decay_block(b):
         start = pl.multiple_of(b * BLOCK, BLOCK)
-        raw = dot(normed[pl.ds(HALO + start, BLOCK), :], step_cols[...])
+        raw = lax.dot_general(
+            normed[pl.ds(HALO + start, BLOCK), :],
+            step_cols[...],
+            (((1,), (1,)), ((), ())),
+            preferred_element_type=F32,
+        )
         step = jnp.maximum(raw, 0.0) + jnp.log1p(jnp.exp(-jnp.abs(raw)))
-        rate_row = jnp.where(first_head, rate[0], rate[1])
-        jump = jumps[pl.ds(start, BLOCK), :]
-        logs = -rate_row * step + jnp.where(first_head, jump[:, 0:1], jump[:, 1:2])
+        rate_row = jnp.where(first_head, rate[:, 0:1], rate[:, 1:2])
+        jump = jumps[:, pl.ds(start, BLOCK)]
+        logs = -rate_row * step + jnp.where(first_rows, jump[0:1, :], jump[1:2, :]).T
         step_b[pl.ds(start, BLOCK), :] = step
         cum_b[pl.ds(start, BLOCK), :] = dot(tri, logs, HIGHEST)
 
@@ -279,31 +365,24 @@
             lax.rem(lane, 2 * QUARTER) < QUARTER, -sine, sine
         )
 
-    other_half = 1 - own_half
-
     def gather_step(s, carry):
-        @pl.when(s < half)
-        def _():
-            for k in range(2):
-                for q in range(2):
-                    for d in range(2):
-                        z_arrival(d, s, k, q).wait_recv()
-                        if q == d:
-                            z_copy(d, s + 1, k, q).start()
-                        else:
-
-                            @pl.when(s + 1 < half)
-                            def _():
-                                z_copy(d, s + 1, k, q).start()
-
-                        y_copy(d, s, k, q, own_half).start()
-
-        @pl.when(s == half)
-        def _():
-            for k in range(2):
-                for d in range(2):
-                    z_arrival(d, s, k, d).wait_recv()
-                    y_copy(d, s, k, d, own_half).start()
+        @pl.when(s > 1)
+        def _():
+            relay(0, s)
+
+        @pl.when(s == 1)
+        def _():
+            if half == 1:
+                relay(0, s)
+            project([me], True)
+
+        @pl.when(s == out_lag)
+        def _():
+            set_off(1)
+
+        @pl.when(s > out_lag)
+        def _():
+            relay(1, s - out_lag)
 
         @pl.when(s <= half)
         def _():
@@ -314,27 +393,22 @@
             decay_block(s - 1)
 
         before = s - 1
+        y_landed(0, before)
 
         @pl.when((before >= 1) & (before < half))
         def _():
-            for d in range(2):
-                for q in range(2):
-                    y_copy(d, before, 0, q, other_half).wait_recv()
-            for d in range(2):
-                project(origin(d, before), False)
+            project([origin(0, before), origin(1, before)], False)
 
         @pl.when(before == half)
         def _():
-            for d in range(2):
-                y_copy(d, before, 0, d, other_half).wait_recv()
-            project(origin(0, before), False)
+            project([origin(0, before)], False)
 
         return carry
 
+    out_lag = max(half + 1 - OUT_EARLY, 1)
     lax.fori_loop(1, half + 2, gather_step, 0)
-    for b in range(half, blocks):
-        if b > half:
-            decay_block(b)
+    for b in range(half + 1, blocks):
+        decay_block(b)
 
     def rotate(x, b):
         start = pl.multiple_of(b * BLOCK, BLOCK)
@@ -466,6 +540,17 @@
         for copy in first_exchange(o):
             copy.start()
 
+    out_next = [half + 2 - out_lag]
+
+    def serve_out(last=False):
+        while out_next[0] <= half:
+            relay(1, out_next[0])
+            out_next[0] += 1
+            if not last:
+                break
+
+    serve_out()
+
     near_mask = half_lanes((BLOCK, LANES))
 
     def local_scan(b, carry):
@@ -491,6 +576,39 @@
         return carry
 
     lax.fori_loop(0, blocks, local_scan, 0)
+
+    serve_out()
+
+    lax.fori_loop(0, blocks, query_block, 0)
+    for d in range(2):
+        kv_copy(d).wait_recv()
+
+    def attend(b, carry):
+        start = pl.multiple_of(b * BLOCK, BLOCK)
+        band = kv_ext[pl.ds(start, 3 * BLOCK), :]
+        row = lax.broadcasted_iota(jnp.int32, (BLOCK, 3 * BLOCK), 0)
+        col = lax.broadcasted_iota(jnp.int32, (BLOCK, 3 * BLOCK), 1)
+        where_key = me * rows - BLOCK + start + col
+        valid = (
+            (jnp.abs(col - BLOCK - row) <= BLOCK) & (where_key >= 0) & (where_key < n * rows)
+        )
+        for h in range(2):
+            query = query_rot[pl.ds(start, BLOCK), h * LANES : (h + 1) * LANES]
+            scores = lax.dot_general(
+                query, band[:, 0:LANES], (((1,), (1,)), ((), ())), preferred_element_type=F32
+            ) * LANES ** (-0.5)
+            masked = jnp.where(valid, scores, -1e30)
+            ceiling = jnp.maximum(jnp.max(masked, axis=-1, keepdims=True), sink[:, h : h + 1])
+            weights = jnp.where(valid, jnp.exp(masked - ceiling), 0.0)
+            bottom = jnp.exp(sink[:, h : h + 1] - ceiling) + jnp.sum(weights, axis=-1, keepdims=True)
+            probs = (weights / bottom).astype(BF16)
+            mix[pl.ds(start, BLOCK), (1 + h) * LANES : (2 + h) * LANES] = dot(
+                probs, band[:, LANES : 2 * LANES]
+            ).astype(BF16)
+        return carry
+
+    lax.fori_loop(0, blocks // 2, attend, 0)
+    serve_out()
 
     for o in order:
         for copy in first_arrival(o):
@@ -525,35 +643,27 @@
     for o in order:
         second_exchange(o).start()
 
-    lax.fori_loop(0, blocks, query_block, 0)
-    for d in range(2):
-        kv_copy(d).wait_recv()
-
-    def attend(b, carry):
-        start = pl.multiple_of(b * BLOCK, BLOCK)
-        band = kv_ext[pl.ds(start, 3 * BLOCK), :]
-        row = lax.broadcasted_iota(jnp.int32, (BLOCK, 3 * BLOCK), 0)
-        col = lax.broadcasted_iota(jnp.int32, (BLOCK, 3 * BLOCK), 1)
-        where_key = me * rows - BLOCK + start + col
-        valid = (
-            (jnp.abs(col - BLOCK - row) <= BLOCK) & (where_key >= 0) & (where_key < n * rows)
-        )
-        for h in range(2):
-            query = query_rot[pl.ds(start, BLOCK), h * LANES : (h + 1) * LANES]
-            scores = lax.dot_general(
-                query, band[:, 0:LANES], (((1,), (1,)), ((), ())), preferred_element_type=F32
-            ) * LANES ** (-0.5)
-            masked = jnp.where(valid, scores, -1e30)
-            ceiling = jnp.maximum(jnp.max(masked, axis=-1, keepdims=True), sink[h])
-            weights = jnp.where(valid, jnp.exp(masked - ceiling), 0.0)
-            bottom = jnp.exp(sink[h] - ceiling) + jnp.sum(weights, axis=-1, keepdims=True)
-            probs = (weights / bottom).astype(BF16)
-            mix[pl.ds(start, BLOCK), (1 + h) * LANES : (2 + h) * LANES] = dot(
-                probs, band[:, LANES : 2 * LANES]
-            ).astype(BF16)
+    serve_out()
+    lax.fori_loop(blocks // 2, blocks, attend, 0)
+    serve_out(True)
+
+    def wait_out(s, carry):
+        y_landed(1, s)
         return carry
 
-    lax.fori_loop(0, blocks, attend, 0)
+    lax.fori_loop(1, half + 1, wait_out, 0)
+
+    def out_weights(i, low, size):
+        return jnp.concatenate(
+            [wout[2 * i, low : low + size, :], wout[2 * i + 1, low : low + size, :]], axis=1
+        )
+
+    def window_product(i, carry):
+        columns = pl.ds(pl.multiple_of(i * 2 * LANES, 2 * LANES), 2 * LANES)
+        part_sum[:, columns] = dot(mix[:, LANES:], out_weights(i, LANES, 2 * LANES))
+        return carry
+
+    lax.fori_loop(0, n // 2, window_product, 0)
 
     for o in order:
         second_arrival(o).wait_recv()
@@ -579,81 +689,88 @@
         mean = jnp.where(near_mask, low, high) * (2.0 / LANES)
         mix[here, 0:LANES] = (gated * lax.rsqrt(mean + 1e-06) * gain[...]).astype(BF16)
 
-    def wait_out(s, carry):
-        @pl.when(s < half)
-        def _():
-            for d in range(2):
-                for q in range(2):
-                    y_copy(d, s, 1, q, other_half).wait_recv()
-
-        @pl.when(s == half)
-        def _():
-            for d in range(2):
-                y_copy(d, s, 1, d, other_half).wait_recv()
-
-        return carry
-
-    lax.fori_loop(1, half + 1, wait_out, 0)
     unit = rows // (2 * nx)
 
-    def rows_for(c):
-        return jnp.concatenate(
-            [
-                mix[pl.ds(pl.multiple_of((2 * x + c) * unit, unit), unit), :]
-                for x in range(nx)
-            ],
-            axis=0,
-        )
-
-    def product(lhs, i):
-        weights = jnp.concatenate([wout[2 * i], wout[2 * i + 1]], axis=1)
-        return dot(lhs, weights).reshape(nx, unit, 2 * LANES)
-
-    def other_product(i, carry):
-        columns = pl.ds(pl.multiple_of(i * 2 * LANES, 2 * LANES), 2 * LANES)
-        pair_out[:, :, columns] = product(rows_for(1 - core), i).astype(BF16)
-        return carry
-
-    def own_product(i, carry):
-        columns = pl.ds(pl.multiple_of(i * 2 * LANES, 2 * LANES), 2 * LANES)
-        own_part[:, :, columns] = product(rows_for(core), i)
-        return carry
+    def group_product(x):
+        first = pl.multiple_of(x * 2 * unit, 2 * unit)
+        theirs = pl.multiple_of((1 - core) * unit, unit)
+        lhs = mix[pl.ds(first, 2 * unit), 0:LANES]
+
+        def tile(i, carry):
+            columns = pl.ds(pl.multiple_of(i * 2 * LANES, 2 * LANES), 2 * LANES)
+            part_sum[pl.ds(first, 2 * unit), columns] += dot(lhs, out_weights(i, 0, LANES))
+            pair_out[x, :, columns] = part_sum[pl.ds(first + theirs, unit), columns].astype(BF16)
+            return carry
+
+        lax.fori_loop(0, n // 2, tile, 0)
 
     def pair_copy(x):
         return pltpu.make_async_remote_copy(
             pair_out.at[x], pair_in.at[x], ps.at[x], pr.at[x], device_id={"tp": partner}
         )
 
-    lax.fori_loop(0, n // 2, other_product, 0)
-    for x in range(nx):
+    x_order = sorted(range(nx), key=lambda o: -min(o, nx - o))
+    groups = [modulo(my_x + o, nx) for o in x_order]
+    for x in groups:
+        group_product(x)
         pair_copy(x).start()
-    lax.fori_loop(0, n // 2, own_product, 0)
-    for x in range(nx):
-        pair_copy(x).wait_recv()
-
-    def group_copy(o):
-        to = modulo(my_x + o, nx)
+
+    side = unit // 2
+
+    def group_sum(x, h):
+        first = pl.multiple_of((2 * x + core) * unit + h * side, side)
+        return part_sum[pl.ds(first, side), :] + pair_in[x, h * side : (h + 1) * side, :].astype(
+            F32
+        )
+
+    next_x, last_x = modulo(my_x + 1, nx), modulo(my_x - 1, nx)
+
+    def x_copy(i, source, target, d):
         return pltpu.make_async_remote_copy(
-            group_out.at[o - 1],
-            group_in.at[o - 1],
-            gs.at[o - 1],
-            gr.at[o - 1],
-            device_id={"tp": 2 * to + core},
-        )
-
-    def group_sum(o):
-        to = modulo(my_x + o, nx)
-        return own_part[to] + pair_in[to].astype(F32)
-
-    x_order = sorted(range(1, nx), key=lambda o: -min(o, nx - o))
-    for o in x_order:
-        group_out[o - 1] = group_sum(o).astype(BF16)
-        group_copy(o).start()
-    mine = group_sum(0)
-    for o in x_order:
-        group_copy(o).wait_recv()
-        mine = mine + group_in[o - 1].astype(F32)
-    result[...] = mine.astype(BF16)
+            source.at[d],
+            target.at[d],
+            gs.at[i, d],
+            gr.at[i, d],
+            device_id={"tp": 2 * (next_x if d == 0 else last_x) + core},
+        )
+
+    def via(d):
+        return x_copy(0, via_out, via_in, d)
+
+    def direct(d):
+        return x_copy(1, direct_out, direct_in, d)
+
+    def merged(d):
+        return x_copy(2, merged_out, merged_in, d)
+
+    beside = (next_x, last_x)
+    if nx == 4:
+        far = modulo(my_x + 2, nx)
+        pair_copy(far).wait_recv()
+        for d in range(2):
+            via_out[d] = group_sum(far, d).astype(BF16)
+            via(d).start()
+    if nx > 1:
+        for x in sorted({0, 1} if nx > 2 else {0}):
+            pair_copy(beside[x]).wait_recv()
+        for d in range(2):
+            direct_out[d] = group_sum(beside[d], 1 - d).astype(BF16)
+            direct(d).start()
+    if nx == 4:
+        for d in range(2):
+            via(d).wait_recv()
+            merged_out[d] = (group_sum(beside[d], d) + via_in[d].astype(F32)).astype(BF16)
+            merged(d).start()
+    pair_copy(my_x).wait_recv()
+    for h in range(2):
+        mine = group_sum(my_x, h)
+        if nx > 1:
+            direct(1 - h).wait_recv()
+            mine = mine + direct_in[1 - h].astype(F32)
+        if nx == 4:
+            merged(h).wait_recv()
+            mine = mine + merged_in[h].astype(F32)
+        result[h * side : (h + 1) * side, :] = mine.astype(BF16)
 
     for d in range(2):
         halo_copy(d).wait_send()
@@ -664,14 +781,18 @@
         second_exchange(o).wait_send()
     for x in range(nx):
         pair_copy(x).wait_send()
-    for o in x_order:
-        group_copy(o).wait_send()
+    for d in range(2):
+        if nx == 4:
+            via(d).wait_send()
+            merged(d).wait_send()
+        if nx > 1:
+            direct(d).wait_send()
 
     def drain(s, carry):
         for k in range(2):
-            for q in range(2):
+            for q in range(pieces[k]):
                 for d in range(2):
-                    if q == d:
+                    if last_way(k, q, d):
                         z_copy(d, s, k, q).wait_send()
                         y_copy(d, s, k, q, own_half).wait_send()
                     else:
@@ -693,23 +814,22 @@
     def shards(*args):
         args = list(args)
         rows, depth = args[0].shape
-        args[1] = args[1].reshape(1, -1)
-        args[9] = args[9].reshape(1, -1)
+        for i in (1, 7, 9, 16):
+            args[i] = args[i].reshape(1, -1)
+        for i in (6, 8):
+            args[i] = args[i].T
         shard = depth // n
         half = n // 2
         blocks = rows // BLOCK
         piece = BLOCK // n
         unit = rows // (2 * nx)
         vmem = pl.BlockSpec(memory_space=pltpu.VMEM)
-        smem = pl.BlockSpec(memory_space=pltpu.SMEM)
-        anywhere = pl.BlockSpec(memory_space=pl.ANY)
-        specs = [vmem] * 19
-        specs[7] = specs[16] = smem
-        for i in (2, 3, 4, 5, 13, 14, 15, 17, 18):
-            specs[i] = anywhere
+        specs = [pl.BlockSpec(memory_space=pl.ANY)] * 19
         dma = pltpu.SemaphoreType.DMA
         V = pltpu.VMEM
-        scratch = [
+        kept = (0, 1, 6, 7, 8, 9, 10, 11, 12, 16)
+        scratch = [V(args[i].shape, args[i].dtype) for i in kept]
+        scratch += [
             V((n, shard, WIN_COLS), BF16),
             V((n, 3 * LANES, LANES), BF16),
             V((rows + 2 * HALO, depth), BF16),
@@ -720,7 +840,7 @@
             V((rows, LANES), F32),
             V((rows, LANES), F32),
             V((rows, LANES), F32),
-            V((depth, LANES), BF16),
+            V((LANES, depth), BF16),
             V((rows, LANES), F32),
             V((rows, LANES), BF16),
             V((rows, LANES), BF16),
@@ -738,16 +858,13 @@
             V((n, 2 * piece, LANES), BF16),
             V((n, 2 * piece, LANES), BF16),
             V((rows, 3 * LANES), BF16),
+            V((rows, depth), F32),
             V((nx, unit, depth), BF16),
             V((nx, unit, depth), BF16),
-            V((nx, unit, depth), F32),
-            V((max(nx - 1, 1), unit, depth), BF16),
-            V((max(nx - 1, 1), unit, depth), BF16),
-            dma((9,)),
-            dma((2, half, 4)),
-            dma((2, half, 4)),
-            dma((2, half, 4)),
-            dma((2, half, 4)),
+            *[V((2, unit // 2, depth), BF16)] * 6,
+            dma((19,)),
+            *[dma((2, half, PIECES))] * 4,
+            *[dma((2, half, 2))] * 4,
             dma((2,)),
             dma((2,)),
             dma((2,)),
@@ -760,8 +877,8 @@
             dma((n,)),
             dma((nx,)),
             dma((nx,)),
-            dma((max(nx - 1, 1),)),
-            dma((max(nx - 1, 1),)),
+            dma((3, 2)),
+            dma((3, 2)),
         ]
         return pl.pallas_call(
             functools.partial(kernel, n, ny, nx),

time: 103 us -> 96.2 us (0.934)
  Pallas kernels: 97.6 us -> 93.8 us
  local copies, waits for them, and re-layouts: 5.05 us -> 1.67 us
    pallas_call x1, Pallas kernels: 97.6 us -> 93.8 us  [shards(): pl.pallas_call(functools.partial(kernel, n, ny, nx), out_shape=jax.ShapeD...]
    unnamed x3 -> x1, local copies, waits for them, and re-layouts: 5.05 us -> 1.67 us
where the time goes in v2:
time: 96.2 us; the launch traced here: 95.5 us
  Pallas kernels  93.8 us (98%)
  local copies, waits for them, and re-layouts  1.67 us (2%)
    pallas_call x1, Pallas kernels, shards(): pl.pallas_call(functools.partial(kernel, n, ny, nx), out_shape=jax.ShapeD...  93.8 us

profile of v2, /device:TPU:1, one launch (start us, length us, event | category | flops | bytes accessed | tf_op | source)
XLA Modules:
  0.0 95.5 jit_solution(16697993556492404349)
XLA Ops:
  0.0 93.8 %shard_map.181 = bf16[64,2048]{1,0:T(8,128)(2,1)} custom-call(bf16[512,2048]{1,0:T(8,128)(2,1)} %tokens_h.1, f32[1,2048]{1,0:T(1,128)} %bitcast.7, bf16[128,128]{1,0:T(8,128)(2,1)} %gate_w.1, bf16[128,128]{1,0:T(8,128)(2,1)} %value_w.1, bf16[128,128]{1,0:T(8,128)(2,1)} %keys_w.1, bf16[128,128]{1,0:T(8,128)(2,1)} %query_w.1, bf16[16,2048]{1,0:T(8,128)(2,1)} %bitcast.6, ...), custom_call_target="tpu_custom_call" | custom-call | tf_op jit(solution)/shard_map/pallas_call | solution.py:883
  93.8 1.7 %copy.21 = bf16[64,2048]{1,0:T(8,128)(2,1)} copy(bf16[64,2048]{1,0:T(8,128)(2,1)} %shard_map.181) | data formatting | bytes 524288

commit v3 on v2

--- a/solution.py
+++ b/solution.py
@@ -13,8 +13,9 @@
 GRID_WIDTH = 64
 QUARTER = 32
 WIN_COLS = 1024
-PIECES = 4
-OUT_EARLY = 3
+PIECES = 2
+TILE = 256
+OUT_LAG = 4
 F32 = jnp.float32
 BF16 = jnp.bfloat16
 HIGHEST = lax.Precision.HIGHEST
@@ -68,6 +69,8 @@
     sink,
     win,
     wout,
+    pwin,
+    pwout,
     normed,
     acc,
     halo_in,
@@ -112,6 +115,16 @@
     czr,
     cys,
     cyr,
+    pzs,
+    pzr,
+    pys,
+    ds,
+    dr,
+    cpzs,
+    cpzr,
+    cpys,
+    cds,
+    cdr,
     hs,
     hr,
     ks,
@@ -170,8 +183,9 @@
         load.start()
 
     barrier = pltpu.get_barrier_semaphore()
-    peers = [{"sp": modulo(me + o, n)} for o in sorted({1, n - 1})]
-    peers += [{"fs": modulo(my_y + o, ny)} for o in sorted({1, ny - 1})]
+    both = (my_tp, partner)
+    peers = [{"sp": modulo(me + o, n), "tp": t} for o in sorted({1, n - 1}) for t in both]
+    peers += [{"fs": modulo(my_y + o, ny), "tp": t} for o in sorted({1, ny - 1}) for t in both]
     peers += [{"tp": partner}]
     peers += [{"tp": 2 * modulo(my_x + o, nx) + core} for o in sorted({1, nx - 1}) if nx > 1]
     for peer in peers:
@@ -190,8 +204,11 @@
             device_id={"sp": right if d == 0 else left},
         )
 
+    relays = core == 1
     buffers = (win, wout)
+    passing = (pwin, pwout)
     pieces = (PIECES, 2)
+    p_sems = ((pzs, pzr, pys, ds, dr, yr), (cpzs, cpzr, cpys, cds, cdr, cyr))
     z_sems = ((zs, zr), (czs, czr))
     y_sems = ((ys, yr), (cys, cyr))
 
@@ -237,49 +254,132 @@
     def last_way(k, q, d):
         return lower(k, q) == (d == 0)
 
+    def p_slab(k, source, q):
+        size = buffers[k].shape[1] // (2 * pieces[k])
+        return passing[k].at[source, pl.ds(q * size, size)]
+
+    def along(d):
+        return right if d == 0 else left
+
+    def p_first(d, k, q):
+        return pltpu.make_async_remote_copy(
+            slab(k, me, own_half, q),
+            p_slab(k, me, q),
+            p_sems[k][0].at[d, 0, q],
+            p_sems[k][1].at[d, 0, q],
+            device_id={"sp": along(d), "tp": partner},
+        )
+
+    def p_move(d, s, k, q, source):
+        ref = p_slab(k, source, q)
+        return pltpu.make_async_remote_copy(
+            ref,
+            ref,
+            p_sems[k][0].at[d, s - 1, q],
+            p_sems[k][1].at[d, s - 1, q],
+            device_id={"sp": along(d)},
+        )
+
+    def p_copy(d, s, k, q):
+        return p_move(d, s, k, q, origin(d, s - 1))
+
+    def p_arrival(d, s, k, q):
+        return p_move(d, s, k, q, origin(d, s))
+
+    def p_side(d, s, k, q):
+        source = origin(d, s)
+        return pltpu.make_async_remote_copy(
+            p_slab(k, source, q),
+            slab(k, source, own_half, q),
+            p_sems[k][2].at[d, s - 1, q],
+            p_sems[k][5].at[d, s - 1, q],
+            device_id={"fs": up if lower(k, q) else down, "tp": partner},
+        )
+
+    def p_down(d, s, k, q):
+        source = origin(d, s)
+        return pltpu.make_async_remote_copy(
+            p_slab(k, source, q),
+            slab(k, source, own_half, q),
+            p_sems[k][3].at[d, s - 1, q],
+            p_sems[k][4].at[d, s - 1, q],
+            device_id={"tp": partner},
+        )
+
+    def first_pieces(k):
+        return [
+            (d, q)
+            for q in range(pieces[k])
+            for d in range(2)
+            if half > 1 or last_way(k, q, d)
+        ]
+
     def set_off(k):
+        @pl.when(relays)
+        def _():
+            for d, q in first_pieces(k):
+                z_copy(d, 1, k, q).start()
+
+        @pl.when(jnp.logical_not(relays))
+        def _():
+            for d, q in first_pieces(k):
+                p_first(d, k, q).start()
+
+    def pass_on(k, s, q, d):
+        for arrival, onward, others in (
+            (z_arrival, z_copy, (lambda *at: y_copy(*at, own_half),)),
+            (p_arrival, p_copy, (p_side, p_down)),
+        ):
+            arrival(d, s, k, q).wait_recv()
+            if last_way(k, q, d):
+
+                @pl.when(s < half)
+                def _():
+                    onward(d, s + 1, k, q).start()
+            else:
+
+                @pl.when(s + 1 < half)
+                def _():
+                    onward(d, s + 1, k, q).start()
+
+            for other in others:
+                other(d, s, k, q).start()
+
+    def relay_piece(k, s, q):
+        @pl.when(relays & (s >= 1) & (s <= half))
+        def _():
+            for d in range(2):
+                if last_way(k, q, d):
+                    pass_on(k, s, q, d)
+                else:
+
+                    @pl.when(s < half)
+                    def _():
+                        pass_on(k, s, q, d)
+
+    def relay(k, s):
         for q in range(pieces[k]):
-            for d in range(2):
-                if half > 1 or last_way(k, q, d):
-                    z_copy(d, 1, k, q).start()
-
-    def relay(k, s):
-        @pl.when(s < half)
-        def _():
-            for q in range(pieces[k]):
-                for d in range(2):
-                    z_arrival(d, s, k, q).wait_recv()
-                    if last_way(k, q, d):
-                        z_copy(d, s + 1, k, q).start()
-                    else:
-
-                        @pl.when(s + 1 < half)
-                        def _():
-                            z_copy(d, s + 1, k, q).start()
-
-                    y_copy(d, s, k, q, own_half).start()
-
-        @pl.when(s == half)
+            relay_piece(k, s, q)
+
+    def y_landed(k, s):
+        def landed(d, q):
+            y_copy(d, s, k, q, 1 - own_half).wait_recv()
+
+            @pl.when(jnp.logical_not(relays))
+            def _():
+                p_down(d, s, k, q).wait_recv()
+
+        @pl.when((s >= 1) & (s <= half))
         def _():
             for q in range(pieces[k]):
                 for d in range(2):
                     if last_way(k, q, d):
-                        z_arrival(d, s, k, q).wait_recv()
-                        y_copy(d, s, k, q, own_half).start()
-
-    def y_landed(k, s):
-        @pl.when((s >= 1) & (s < half))
-        def _():
-            for q in range(pieces[k]):
-                for d in range(2):
-                    y_copy(d, s, k, q, 1 - own_half).wait_recv()
-
-        @pl.when(s == half)
-        def _():
-            for q in range(pieces[k]):
-                for d in range(2):
-                    if last_way(k, q, d):
-                        y_copy(d, s, k, q, 1 - own_half).wait_recv()
+                        landed(d, q)
+                    else:
+
+                        @pl.when(s < half)
+                        def _():
+                            landed(d, q)
 
     set_off(0)
     for load in late_loads:
@@ -297,10 +397,21 @@
         normed[pl.ds(HALO + start, 32), :] = normalise(tokens[pl.ds(start, 32), :])
         return carry
 
-    lax.fori_loop(0, rows // 64, normalise_chunk, 0)
-    if half > 1:
-        relay(0, 1)
-    lax.fori_loop(rows // 64, rows // 32, normalise_chunk, 0)
+    chunks = rows // 32
+    early = chunks - 2 * PIECES if chunks > 2 * PIECES else 0
+    lax.fori_loop(0, early, normalise_chunk, 0)
+
+    def normalise_late(i, carry):
+        for q in range(PIECES):
+
+            @pl.when(i == q)
+            def _():
+                relay_piece(0, 1, q)
+
+        each = (chunks - early) // PIECES
+        return lax.fori_loop(early + i * each, early + (i + 1) * each, normalise_chunk, carry)
+
+    lax.fori_loop(0, PIECES, normalise_late, 0)
     for d in range(2):
         halo_copy(d).wait_recv()
         normed[(0 if d == 0 else HALO + rows) : (HALO if d == 0 else 2 * HALO + rows), :] = (
@@ -310,15 +421,18 @@
     def slice_of(source):
         return normed[:, pl.ds(pl.multiple_of(source * shard, shard), shard)]
 
-    def project(sources, first):
-        for c in range(0, WIN_COLS, 256):
-            term = functools.reduce(
-                jnp.add, [dot(slice_of(o), win[o, :, c : c + 256]) for o in sources]
-            )
-            if first:
-                acc[:, c : c + 256] = term
-            else:
-                acc[:, c : c + 256] += term
+    def project(sources, tile, first):
+        columns = slice(tile * TILE, (tile + 1) * TILE)
+        term = functools.reduce(
+            jnp.add, [dot(slice_of(o), win[o, :, columns]) for o in sources]
+        )
+        if first:
+            acc[:, columns] = term
+        else:
+            acc[:, columns] += term
+
+    for tile in range(WIN_COLS // TILE):
+        project([me], tile, True)
 
     heads = lax.broadcasted_iota(jnp.int32, (LANES, step_w.shape[0]), 1)
     lanes_of = lax.broadcasted_iota(jnp.int32, (LANES, step_w.shape[0]), 0)
@@ -365,48 +479,45 @@
             lax.rem(lane, 2 * QUARTER) < QUARTER, -sine, sine
         )
 
+    out_lag = OUT_LAG if half > OUT_LAG else 1
+
     def gather_step(s, carry):
-        @pl.when(s > 1)
-        def _():
-            relay(0, s)
-
-        @pl.when(s == 1)
-        def _():
-            if half == 1:
-                relay(0, s)
-            project([me], True)
-
-        @pl.when(s == out_lag)
+        @pl.when(s == out_lag + 1)
         def _():
             set_off(1)
 
-        @pl.when(s > out_lag)
-        def _():
-            relay(1, s - out_lag)
-
-        @pl.when(s <= half)
-        def _():
-            angle_block(s - 1)
-
-        @pl.when(s <= blocks)
-        def _():
-            decay_block(s - 1)
-
-        before = s - 1
-        y_landed(0, before)
-
-        @pl.when((before >= 1) & (before < half))
-        def _():
-            project([origin(0, before), origin(1, before)], False)
-
-        @pl.when(before == half)
-        def _():
-            project([origin(0, before)], False)
+        before = s - 2
+        for q in range(WIN_COLS // TILE):
+            if q % 2 == 0:
+                relay_piece(0, s, q // 2)
+            else:
+                relay_piece(1, s - 1 - out_lag, q // 2)
+            if q == 0:
+                y_landed(0, before)
+
+            @pl.when((before >= 1) & (before < half))
+            def _():
+                project([origin(0, before), origin(1, before)], q, False)
+
+            @pl.when(before == half)
+            def _():
+                project([origin(0, before)], q, False)
+
+            if q == 1:
+
+                @pl.when(s - 1 <= half)
+                def _():
+                    angle_block(s - 2)
+
+            if q == 2:
+
+                @pl.when(s - 1 <= blocks)
+                def _():
+                    decay_block(s - 2)
 
         return carry
 
-    out_lag = max(half + 1 - OUT_EARLY, 1)
-    lax.fori_loop(1, half + 2, gather_step, 0)
+    lax.fori_loop(2, half + 3, gather_step, 0)
     for b in range(half + 1, blocks):
         decay_block(b)
 
@@ -577,8 +688,6 @@
 
     lax.fori_loop(0, blocks, local_scan, 0)
 
-    serve_out()
-
     lax.fori_loop(0, blocks, query_block, 0)
     for d in range(2):
         kv_copy(d).wait_recv()
@@ -610,6 +719,8 @@
     lax.fori_loop(0, blocks // 2, attend, 0)
     serve_out()
 
+    lax.fori_loop(blocks // 2, blocks, attend, 0)
+
     for o in order:
         for copy in first_arrival(o):
             copy.wait_recv()
@@ -643,8 +754,6 @@
     for o in order:
         second_exchange(o).start()
 
-    serve_out()
-    lax.fori_loop(blocks // 2, blocks, attend, 0)
     serve_out(True)
 
     def wait_out(s, carry):
@@ -658,12 +767,16 @@
             [wout[2 * i, low : low + size, :], wout[2 * i + 1, low : low + size, :]], axis=1
         )
 
+    spread_tiles = 4 if n % 8 == 0 else 1
+
     def window_product(i, carry):
-        columns = pl.ds(pl.multiple_of(i * 2 * LANES, 2 * LANES), 2 * LANES)
-        part_sum[:, columns] = dot(mix[:, LANES:], out_weights(i, LANES, 2 * LANES))
+        for u in range(spread_tiles):
+            t = i * spread_tiles + u
+            columns = pl.ds(pl.multiple_of(t * 2 * LANES, 2 * LANES), 2 * LANES)
+            part_sum[:, columns] = dot(mix[:, LANES:], out_weights(t, LANES, 2 * LANES))
         return carry
 
-    lax.fori_loop(0, n // 2, window_product, 0)
+    lax.fori_loop(0, n // 2 // spread_tiles, window_product, 0)
 
     for o in order:
         second_arrival(o).wait_recv()
@@ -695,25 +808,23 @@
         first = pl.multiple_of(x * 2 * unit, 2 * unit)
         theirs = pl.multiple_of((1 - core) * unit, unit)
         lhs = mix[pl.ds(first, 2 * unit), 0:LANES]
-
-        def tile(i, carry):
-            columns = pl.ds(pl.multiple_of(i * 2 * LANES, 2 * LANES), 2 * LANES)
-            part_sum[pl.ds(first, 2 * unit), columns] += dot(lhs, out_weights(i, 0, LANES))
-            pair_out[x, :, columns] = part_sum[pl.ds(first + theirs, unit), columns].astype(BF16)
-            return carry
-
-        lax.fori_loop(0, n // 2, tile, 0)
+        for t in range(n // 2):
+            columns = slice(t * 2 * LANES, (t + 1) * 2 * LANES)
+            part_sum[pl.ds(first, 2 * unit), columns] += dot(lhs, out_weights(t, 0, LANES))
+        pair_out[x] = part_sum[pl.ds(first + theirs, unit), :].astype(BF16)
 
     def pair_copy(x):
         return pltpu.make_async_remote_copy(
             pair_out.at[x], pair_in.at[x], ps.at[x], pr.at[x], device_id={"tp": partner}
         )
 
-    x_order = sorted(range(nx), key=lambda o: -min(o, nx - o))
-    groups = [modulo(my_x + o, nx) for o in x_order]
-    for x in groups:
+    def group_step(i, carry):
+        x = modulo(my_x + nx // 2 + i * (nx - 1), nx)
         group_product(x)
         pair_copy(x).start()
+        return carry
+
+    lax.fori_loop(0, nx, group_step, 0)
 
     side = unit // 2
 
@@ -744,6 +855,7 @@
         return x_copy(2, merged_out, merged_in, d)
 
     beside = (next_x, last_x)
+
     if nx == 4:
         far = modulo(my_x + 2, nx)
         pair_copy(far).wait_recv()
@@ -789,22 +901,38 @@
             direct(d).wait_send()
 
     def drain(s, carry):
+        def left(k, q, d):
+            @pl.when(relays)
+            def _():
+                z_copy(d, s, k, q).wait_send()
+                y_copy(d, s, k, q, own_half).wait_send()
+                p_side(d, s, k, q).wait_send()
+                p_down(d, s, k, q).wait_send()
+
+                @pl.when(s > 1)
+                def _():
+                    p_copy(d, s, k, q).wait_send()
+
         for k in range(2):
             for q in range(pieces[k]):
                 for d in range(2):
                     if last_way(k, q, d):
-                        z_copy(d, s, k, q).wait_send()
-                        y_copy(d, s, k, q, own_half).wait_send()
+                        left(k, q, d)
                     else:
 
                         @pl.when(s < half)
                         def _():
-                            z_copy(d, s, k, q).wait_send()
-                            y_copy(d, s, k, q, own_half).wait_send()
+                            left(k, q, d)
 
         return carry
 
     lax.fori_loop(1, half + 1, drain, 0)
+
+    @pl.when(jnp.logical_not(relays))
+    def _():
+        for k in range(2):
+            for d, q in first_pieces(k):
+                p_first(d, k, q).wait_send()
 
 
 def solution(mesh):
@@ -832,6 +960,8 @@
         scratch += [
             V((n, shard, WIN_COLS), BF16),
             V((n, 3 * LANES, LANES), BF16),
+            V((n, shard // 2, WIN_COLS), BF16),
+            V((n, 3 * LANES // 2, LANES), BF16),
             V((rows + 2 * HALO, depth), BF16),
             V((rows + 2 * HALO, WIN_COLS), F32),
             V((2, HALO, depth), BF16),
@@ -865,6 +995,8 @@
             dma((19,)),
             *[dma((2, half, PIECES))] * 4,
             *[dma((2, half, 2))] * 4,
+            *[dma((2, half, PIECES))] * 5,
+            *[dma((2, half, 2))] * 5,
             dma((2,)),
             dma((2,)),
             dma((2,)),

time: 96.2 us -> 89.4 us (0.929)
  Pallas kernels: 93.8 us -> 87.5 us
    pallas_call x1, Pallas kernels: 93.8 us -> 87.5 us  [shards(): pl.pallas_call(functools.partial(kernel, n, ny, nx), out_shape=jax.ShapeD...]
where the time goes in v3:
time: 89.4 us; the launch traced here: 89.2 us
  Pallas kernels  87.5 us (98%)
  local copies, waits for them, and re-layouts  1.67 us (2%)
    pallas_call x1, Pallas kernels, shards(): pl.pallas_call(functools.partial(kernel, n, ny, nx), out_shape=jax.ShapeD...  87.5 us

profile of v3, /device:TPU:1, one launch (start us, length us, event | category | flops | bytes accessed | tf_op | source)
XLA Modules:
  0.0 89.2 jit_solution(10898842495750751129)
XLA Ops:
  0.0 87.5 %shard_map.181 = bf16[64,2048]{1,0:T(8,128)(2,1)} custom-call(bf16[512,2048]{1,0:T(8,128)(2,1)} %tokens_h.1, f32[1,2048]{1,0:T(1,128)} %bitcast.7, bf16[128,128]{1,0:T(8,128)(2,1)} %gate_w.1, bf16[128,128]{1,0:T(8,128)(2,1)} %value_w.1, bf16[128,128]{1,0:T(8,128)(2,1)} %keys_w.1, bf16[128,128]{1,0:T(8,128)(2,1)} %query_w.1, bf16[16,2048]{1,0:T(8,128)(2,1)} %bitcast.6, ...), custom_call_target="tpu_custom_call" | custom-call | tf_op jit(solution)/shard_map/pallas_call | solution.py:1015
  87.5 1.7 %copy.21 = bf16[64,2048]{1,0:T(8,128)(2,1)} copy(bf16[64,2048]{1,0:T(8,128)(2,1)} %shard_map.181) | data formatting | bytes 524288
